TPU v7x, 128 devices: a whole 4x4x4 slice. The times are simulated.
128 devices in a mesh: dp: 4 (over x), kv: 16 (over z, y), tp: 2 (over core).
Axes of the slice: x: 4, y: 4, z: 4, core: 2. Of those that a mesh axis runs over, the one named last changes fastest.
Arguments:
- tokens: bfloat16 [512, 2048], P('dp', ('kv', 'tp')), may hold values from -100 to 100
- delta_state: float32 [512, 8, 128, 128], P(('dp', 'kv'), 'tp'), may hold values from -0.6 to 0.6
- gain_in: bfloat16 [2048], P('kv'), may hold values from 0.099609375 to 1.8984375
- w_query: bfloat16 [2048, 1024], P('kv', 'tp'), may hold values from -0.125 to 0.125
- w_key: bfloat16 [2048, 1024], P('kv', 'tp'), may hold values from -0.125 to 0.125
- w_value: bfloat16 [2048, 1024], P('kv', 'tp'), may hold values from -0.125 to 0.125
- w_out_gate: bfloat16 [2048, 1024], P('kv', 'tp'), may hold values from -0.125 to 0.125
- w_beta: bfloat16 [2048, 8], P('kv'), may hold values from -0.125 to 0.125
- w_decay: bfloat16 [2048, 8], P('kv'), may hold values from -0.125 to 0.125
- decay_rate: float32 [8], P('tp'), may hold values from 0.05 to 3
- head_gain: float32 [128], replicated, may hold values from 0.1 to 1.9
- w_mix: bfloat16 [1024, 2048], P('tp', 'kv'), may hold values from -0.1875 to 0.1875
- gain_mid: bfloat16 [2048], P('kv'), may hold values from 0.099609375 to 1.8984375
- w_gate: bfloat16 [2048, 5632], P('tp', 'kv'), may hold values from -0.125 to 0.125
- w_up: bfloat16 [2048, 5632], P('tp', 'kv'), may hold values from -0.125 to 0.125
- w_down: bfloat16 [5632, 2048], P('kv', 'tp'), may hold values from -0.078125 to 0.078125
Outputs:
- layer_out: bfloat16 [512, 2048], P('dp', ('kv', 'tp'))
- next_state: float32 [512, 8, 128, 128], P(('dp', 'kv'), 'tp')
All inputs are finite; a program needn't handle non-finite values.
Results may differ from a plain program's by a relative error of at most 0.0095.
Values may be sent and summed in bfloat16 or wider, within the bound.
No kernel may reach another device: no remote copies, remote signals or barrier semaphores. Data moves between devices by JAX's collectives and lax.ppermute only.
A program may use at most 64 MiB of HBM per device.

v0:
```python
import jax
import jax.numpy as jnp
from jax import lax
from jax.sharding import Mesh
from jax.sharding import PartitionSpec as P

D = 2048
HEAD_DIM = 128
KV = ("kv_0", "kv_1")
KV_TP = ("kv_0", "kv_1", "tp")
DP_KV = ("dp", "kv_0", "kv_1")


norm_epsilon = 1e-06


def from_everyone(array, axis):
    copies = jnp.broadcast_to(array, (lax.axis_size(axis), *array.shape))
    return lax.all_to_all(copies, axis, split_axis=0, concat_axis=0, tiled=True)


def joined_along(tiles, dim):
    tiles = jnp.moveaxis(tiles, 0, dim)
    lengths = tiles.shape
    return tiles.reshape(*lengths[:dim], lengths[dim] * lengths[dim + 1], *lengths[dim + 2 :])


def collect(array, axis, dim):
    tiles = from_everyone(array, axis)
    return joined_along(tiles, dim)


def by_axis(array, axes):
    for axis in axes:
        array = lax.psum(array, axis)
    return array


def split_up(array, dim, devices):
    lengths = array.shape
    tiles = array.reshape(*lengths[:dim], devices, lengths[dim] // devices, *lengths[dim + 1 :])
    return jnp.moveaxis(tiles, dim, 0)


def sum_at_owner(array, axis, dim):
    devices = lax.axis_size(axis)
    tiles = lax.all_to_all(split_up(array, dim, devices), axis, 0, 0, tiled=True)
    return jnp.sum(tiles.astype(jnp.float32), axis=0)


def total_of_pieces(array, axis):
    return lax.all_gather(array, axis).sum(0)


def taken_together(array, axis):
    everything = from_everyone(array, axis)
    return jnp.sum(everything.astype(jnp.float32), axis=0)


def unit_rows(vector):
    return vector * lax.rsqrt(jnp.sum(vector * vector, axis=-1, keepdims=True) + norm_epsilon)


def mixer_core(
    query_lin, key_lin, value_lin, gate_lin, beta_lin, decay_lin, delta_state, decay_rate, head_gain
):
    seq_count = query_lin.shape[0]
    head_count = beta_lin.shape[1]
    shaped = lambda matrix: matrix.reshape(seq_count, head_count, HEAD_DIM)
    query = unit_rows(jax.nn.silu(shaped(query_lin))) * HEAD_DIM ** (-0.5)
    key_vec = unit_rows(jax.nn.silu(shaped(key_lin)))
    value_vec = jax.nn.silu(shaped(value_lin))
    write_rate = jax.nn.sigmoid(beta_lin)
    keep_rate = jnp.exp(-decay_rate[None, :] * jax.nn.softplus(decay_lin))
    recalled = jnp.einsum("bhkv,bhk->bhv", delta_state, key_vec)
    correction = write_rate[..., None] * (value_vec - keep_rate[..., None] * recalled)
    next_state = (
        keep_rate[..., None, None] * delta_state + key_vec[..., :, None] * correction[..., None, :]
    )
    readout = jnp.einsum("bhkv,bhk->bhv", next_state, query)
    readout = readout * lax.rsqrt(
        jnp.mean(readout * readout, axis=-1, keepdims=True) + norm_epsilon
    )
    readout = readout * head_gain * jax.nn.silu(shaped(gate_lin))
    return (readout.reshape(seq_count, head_count * HEAD_DIM).astype(jnp.bfloat16), next_state)


def local(
    tokens,
    delta_state,
    gain_in,
    w_query,
    w_key,
    w_value,
    w_out_gate,
    w_beta,
    w_decay,
    decay_rate,
    head_gain,
    w_mix,
    gain_mid,
    w_gate,
    w_up,
    w_down,
):
    group_size = lax.axis_size(KV)
    group_pos = lax.axis_index(KV)
    core_pos = lax.axis_index("tp")
    all_rows = tokens.shape[0]
    own_rows = all_rows // group_size
    own_first = group_pos * own_rows
    feature_count = tokens.shape[1]
    head_count = w_query.shape[1] // HEAD_DIM
    width_dev = w_query.shape[1]
    token_float = tokens.astype(jnp.float32)
    sum_squares = jnp.sum(token_float * token_float, axis=1, keepdims=True)
    whole_rows, square_pair = (
        collect(tokens, "tp", 1),
        collect(sum_squares.astype(jnp.bfloat16), "tp", 1).astype(sum_squares.dtype),
    )
    square_total = by_axis(jnp.sum(square_pair, axis=1), KV)
    row_scale = lax.rsqrt(square_total / D + norm_epsilon)
    normed = (whole_rows.astype(jnp.float32) * gain_in.astype(jnp.float32)).astype(jnp.bfloat16)
    beta_cols = lax.dynamic_slice_in_dim(w_beta, core_pos * head_count, head_count, 1)
    decay_cols = lax.dynamic_slice_in_dim(w_decay, core_pos * head_count, head_count, 1)
    row_block = normed
    results = [
        jnp.dot(row_block, weight, preferred_element_type=jnp.float32)
        for weight in (w_query, w_key, w_value, w_out_gate, beta_cols, decay_cols)
    ]
    summand = jnp.concatenate(results, axis=1)
    projected = sum_at_owner(summand.astype(jnp.bfloat16), KV, 0)
    projected = projected * lax.dynamic_slice_in_dim(row_scale, own_first, own_rows, 0)[:, None]
    mixed, next_state = mixer_core(
        projected[:, :width_dev],
        projected[:, width_dev : 2 * width_dev],
        projected[:, 2 * width_dev : 3 * width_dev],
        projected[:, 3 * width_dev : 4 * width_dev],
        projected[:, 4 * width_dev : 4 * width_dev + head_count],
        projected[:, 4 * width_dev + head_count :],
        delta_state,
        decay_rate,
        head_gain,
    )
    attn_part = jnp.dot(collect(mixed, KV, 0), w_mix, preferred_element_type=jnp.float32)
    attn = sum_at_owner(attn_part.astype(jnp.bfloat16), "tp", 1)
    middle_own = (token_float + attn).astype(jnp.bfloat16)
    middle_float = middle_own.astype(jnp.float32)
    mid_squares = jnp.sum(middle_float * middle_float, axis=1, keepdims=True)
    gain_own = lax.dynamic_slice_in_dim(gain_mid, core_pos * feature_count, feature_count, 0)
    normed_own = (middle_float * gain_own.astype(jnp.float32)).astype(jnp.bfloat16)
    normed_half, square_parts = (
        collect(normed_own, KV, 1),
        collect(mid_squares.astype(jnp.bfloat16), KV, 1).astype(mid_squares.dtype),
    )
    mid_total = total_of_pieces(jnp.sum(square_parts, axis=1), "tp")
    mid_scale = lax.rsqrt(mid_total / D + norm_epsilon)
    hidden_dev = w_gate.shape[1]
    row_block = normed_half
    summand = jnp.concatenate(
        [
            jnp.dot(row_block, w_gate, preferred_element_type=jnp.float32),
            jnp.dot(row_block, w_up, preferred_element_type=jnp.float32),
        ],
        axis=1,
    )
    gate_up = taken_together(summand.astype(jnp.bfloat16), "tp").astype(jnp.float32)
    gate_up = gate_up * mid_scale[:, None]
    activated = (jax.nn.silu(gate_up[:, :hidden_dev]) * gate_up[:, hidden_dev:]).astype(
        jnp.bfloat16
    )
    down_local = jnp.dot(activated, w_down, preferred_element_type=jnp.float32)
    down_part = sum_at_owner(down_local.astype(jnp.bfloat16), KV, 1)
    layer_out = (middle_float + down_part).astype(jnp.bfloat16)
    return (layer_out, next_state)


def solution(mesh):
    split = Mesh(
        mesh.devices.reshape(mesh.shape["dp"], 4, 4, mesh.shape["tp"]), ("dp", "kv_0", "kv_1", "tp")
    )
    in_specs = (
        P("dp", KV_TP),
        P(DP_KV, "tp", None, None),
        P(KV),
        P(KV, "tp"),
        P(KV, "tp"),
        P(KV, "tp"),
        P(KV, "tp"),
        P(KV, None),
        P(KV, None),
        P("tp"),
        P(),
        P("tp", KV),
        P(KV),
        P("tp", KV),
        P("tp", KV),
        P(KV, "tp"),
    )
    out_specs = (P("dp", KV_TP), P(DP_KV, "tp", None, None))
    return jax.shard_map(local, mesh=split, in_specs=in_specs, out_specs=out_specs, check_vma=False)
```

profile of v0, /device:TPU:1, one launch (start us, length us, event | category | flops | bytes accessed | tf_op | source)
XLA Modules:
  0.0 113.0 jit_solution(5233247523237821783)
XLA Ops:
  0.6 1.4 %broadcast_in_dim.12 = bf16[2,128,64]{1,2,0:T(8,128)(2,1)} broadcast(bf16[128,64]{0,1:T(8,128)(2,1)} %param.16), dimensions={1,2} | broadcast | bytes 49152 | tf_op jit(solution)/shard_map/broadcast_in_dim | solution.py:18
  2.1 4.6 %all-to-all-start = ((bf16[2,128,64]{1,2,0:T(8,128)(2,1)}), bf16[2,128,64]{1,2,0:T(8,128)(2,1)S(1)}, u32[]{:S(2)}, u32[]{:S(2)}) async-start(bf16[2,128,64]{1,2,0:T(8,128)(2,1)} %broadcast_in_dim.12), calls=%async_computation | async-start | bytes 65536 | tf_op jit(solution)/shard_map/all_to_all | solution.py:19
  8.6 3.2 %all-to-all-start.2 = ((bf16[2,128,1]{1,2,0:T(2,128)(2,1)}), bf16[2,128,1]{1,2,0:T(2,128)(2,1)S(1)}, u32[]{:S(2)}, u32[]{:S(2)}) async-start(bf16[2,128,1]{1,2,0:T(2,128)(2,1)} %broadcast_in_dim.13), calls=%async_computation.2 | async-start | bytes 2048 | tf_op jit(solution)/shard_map/all_to_all | solution.py:19
  12.1 0.9 fusion.29
  13.2 0.9 fusion.31
  14.5 1.1 convolution_convert_fusion.1
  15.6 1.2 %convolution_convert_fusion.2 = bf16[16,8,512]{2,1,0:T(8,128)(2,1)S(1)} fusion(bf16[16,8,128]{2,1,0:T(8,128)(2,1)S(1)} %multiply_convert_fusion, bf16[128,512]{1,0:T(8,128)(2,1)} %param.21), kind=kOutput, calls=%fused_computation.3 | convolution fusion | flops 16842752 | bytes 294912 | tf_op jit(solution)/shard_map/dot_general | solution.py:128
  16.8 1.1 convolution_convert_fusion.3
  17.9 1.1 convolution_convert_fusion.4
  19.0 0.9 concatenate.9
  19.9 7.9 %all-to-all-start.1 = ((bf16[16,8,2056]{2,1,0:T(8,128)(2,1)}), bf16[16,8,2056]{2,1,0:T(8,128)(2,1)S(1)}, u32[]{:S(2)}, u32[]{:S(2)}) async-start(bf16[16,8,2056]{2,1,0:T(8,128)(2,1)} %concatenate.9), calls=%async_computation.1 | async-start | bytes 1114112 | tf_op jit(solution)/shard_map/all_to_all | solution.py:47
  27.9 9.9 %psum.14 = f32[128]{0:T(128)S(1)} all-reduce(f32[128]{0:T(128)S(1)} %convert_reduce_fusion.5), channel_id=1, replica_groups=mesh['dp'=4,'kv_0'=4,'kv_1'=4,'tp'=2] {'kv_0'}, use_global_device_ids=true, to_apply=%region_3.0 | all-reduce | flops 128 | bytes 1024 | tf_op jit(solution)/shard_map/psum | solution.py:35
  37.7 10.8 %psum.15 = f32[128]{0:T(128)S(1)} all-reduce(f32[128]{0:T(128)S(1)} %psum.14), channel_id=1, replica_groups=mesh['dp'=4,'kv_0'=4,'kv_1'=4,'tp'=2] {'kv_1'}, use_global_device_ids=true, to_apply=%region_4.0 | all-reduce | flops 128 | bytes 1024 | tf_op jit(solution)/shard_map/psum | solution.py:35
  50.6 1.3 %copy-done.2 = f32[8,4,128,128]{3,2,1,0:T(8,128)} copy-done((f32[8,4,128,128]{3,2,1,0:T(8,128)}, f32[8,4,128,128]{3,2,1,0:T(8,128)S(1)}, u32[]{:S(2)}) %copy-start.2) | copy-done | bytes 2097176
  53.3 3.5 %all-to-all-start.3 = ((bf16[16,8,512]{2,1,0:T(8,128)(2,1)}), bf16[16,8,512]{2,1,0:T(8,128)(2,1)S(1)}, u32[]{:S(2)}, u32[]{:S(2)}) async-start(bf16[16,8,512]{2,1,0:T(8,128)(2,1)} %broadcast_in_dim.14), calls=%async_computation.3 | async-start | bytes 262144 | tf_op jit(solution)/shard_map/all_to_all | solution.py:19
  56.9 6.7 %all-to-all-done.3 = bf16[16,8,512]{2,1,0:T(8,128)(2,1)S(1)} async-done(((bf16[16,8,512]{2,1,0:T(8,128)(2,1)}), bf16[16,8,512]{2,1,0:T(8,128)(2,1)S(1)}, u32[]{:S(2)}, u32[]{:S(2)}) %all-to-all-start.3) | async-done | bytes 131104 | tf_op jit(solution)/shard_map/all_to_all | solution.py:19
  63.9 7.8 %all_to_all.45 = bf16[2,128,64]{1,2,0:T(8,128)(2,1)S(1)} all-to-all(bf16[2,128,64]{1,2,0:T(8,128)(2,1)S(1)} %bitcast.103), channel_id=1, replica_groups=mesh['dp'=4,'kv_0'=4,'kv_1'=4,'tp'=2] {'tp'}, dimensions={0} | all-to-all | bytes 65536 | tf_op jit(solution)/shard_map/all_to_all | solution.py:47
  72.4 3.5 %all-to-all-start.7 = ((bf16[16,128,1]{1,2,0:T(2,128)(2,1)}), bf16[16,128,1]{1,2,0:T(2,128)(2,1)S(1)}, u32[]{:S(2)}, u32[]{:S(2)}) async-start(bf16[16,128,1]{1,2,0:T(2,128)(2,1)} %broadcast_in_dim.17), calls=%async_computation.7 | async-start | bytes 16384 | tf_op jit(solution)/shard_map/all_to_all | solution.py:19
  75.9 6.2 %all-to-all-done.7 = bf16[16,128,1]{1,2,0:T(2,128)(2,1)S(1)} async-done(((bf16[16,128,1]{1,2,0:T(2,128)(2,1)}), bf16[16,128,1]{1,2,0:T(2,128)(2,1)S(1)}, u32[]{:S(2)}, u32[]{:S(2)}) %all-to-all-start.7) | async-done | bytes 4128 | tf_op jit(solution)/shard_map/all_to_all | solution.py:19
  82.9 3.5 %all-to-all-start.5 = ((bf16[16,128,64]{1,2,0:T(8,128)(2,1)}), bf16[16,128,64]{1,2,0:T(8,128)(2,1)S(1)}, u32[]{:S(2)}, u32[]{:S(2)}) async-start(bf16[16,128,64]{1,2,0:T(8,128)(2,1)} %broadcast_in_dim.15), calls=%async_computation.5 | async-start | bytes 524288 | tf_op jit(solution)/shard_map/all_to_all | solution.py:19
  86.5 3.0 %all-gather.1 = f32[2,1,128]{2,1,0:T(1,128)S(1)} all-gather(f32[1,1,128]{2,1,0:T(1,128)S(1)} %bitcast.104), channel_id=2, replica_groups=mesh['dp'=4,'kv_0'=4,'kv_1'=4,'tp'=2] {'tp'}, dimensions={0}, use_global_device_ids=true | all-gather | bytes 1536 | tf_op jit(solution)/shard_map/all_gather | solution.py:52
  89.4 4.5 %all-to-all-done.5 = bf16[16,128,64]{1,2,0:T(8,128)(2,1)S(1)} async-done(((bf16[16,128,64]{1,2,0:T(8,128)(2,1)}), bf16[16,128,64]{1,2,0:T(8,128)(2,1)S(1)}, u32[]{:S(2)}, u32[]{:S(2)}) %all-to-all-start.5) | async-done | bytes 262176 | tf_op jit(solution)/shard_map/all_to_all | solution.py:19
  94.7 6.3 %all_to_all.46 = bf16[2,128,704]{1,2,0:T(8,128)(2,1)S(1)} all-to-all(bf16[2,128,704]{1,2,0:T(8,128)(2,1)S(1)} %broadcast_in_dim.16), channel_id=1, replica_groups=mesh['dp'=4,'kv_0'=4,'kv_1'=4,'tp'=2] {'tp'}, dimensions={0} | all-to-all | bytes 720896 | tf_op jit(solution)/shard_map/all_to_all | solution.py:19
  101.6 10.8 %all_to_all.47 = bf16[16,128,64]{1,2,0:T(8,128)(2,1)S(1)} all-to-all(bf16[16,128,64]{1,2,0:T(8,128)(2,1)S(1)} %bitcast.102), channel_id=1, replica_groups=mesh['dp'=4,'kv_0'=4,'kv_1'=4,'tp'=2] {'kv_0','kv_1'}, dimensions={0} | all-to-all | bytes 524288 | tf_op jit(solution)/shard_map/all_to_all | solution.py:47
  (77 shorter events, 10.1 us)
Async XLA Ops:
  0.6 100.4 %copy-start = (bf16[352,1024]{1,0:T(8,128)(2,1)S(1)}, bf16[352,1024]{1,0:T(8,128)(2,1)}, u32[]{:S(2)}) copy-start(bf16[352,1024]{1,0:T(8,128)(2,1)} %param.31) | copy-start | bytes 2162692
  2.1 6.0 %all-to-all-start = ((bf16[2,128,64]{1,2,0:T(8,128)(2,1)}), bf16[2,128,64]{1,2,0:T(8,128)(2,1)S(1)}, u32[]{:S(2)}, u32[]{:S(2)}) async-start(bf16[2,128,64]{1,2,0:T(8,128)(2,1)} %broadcast_in_dim.12), calls=%async_computation | async-start | bytes 65536 | tf_op jit(solution)/shard_map/all_to_all | solution.py:19
  8.6 11.3 %all-to-all-start.2 = ((bf16[2,128,1]{1,2,0:T(2,128)(2,1)}), bf16[2,128,1]{1,2,0:T(2,128)(2,1)S(1)}, u32[]{:S(2)}, u32[]{:S(2)}) async-start(bf16[2,128,1]{1,2,0:T(2,128)(2,1)} %broadcast_in_dim.13), calls=%async_computation.2 | async-start | bytes 2048 | tf_op jit(solution)/shard_map/all_to_all | solution.py:19
  11.9 16.0 %copy-start.8 = (f32[4]{0:T(128)S(1)}, f32[4]{0:T(128)}, u32[]{:S(2)}) copy-start(f32[4]{0:T(128)} %param.25) | copy-start | bytes 52
  15.6 33.8 %copy-start.1 = (f32[8,4,128,128]{3,2,1,0:T(8,128)S(1)}, f32[8,4,128,128]{3,2,1,0:T(8,128)}, u32[]{:S(2)}) copy-start(f32[8,4,128,128]{3,2,1,0:T(8,128)} %param.17) | copy-start | bytes 6291460
  19.9 28.6 %all-to-all-start.1 = ((bf16[16,8,2056]{2,1,0:T(8,128)(2,1)}), bf16[16,8,2056]{2,1,0:T(8,128)(2,1)S(1)}, u32[]{:S(2)}, u32[]{:S(2)}) async-start(bf16[16,8,2056]{2,1,0:T(8,128)(2,1)} %concatenate.9), calls=%async_computation.1 | async-start | bytes 1114112 | tf_op jit(solution)/shard_map/all_to_all | solution.py:47
  50.6 1.3 %copy-start.2 = (f32[8,4,128,128]{3,2,1,0:T(8,128)}, f32[8,4,128,128]{3,2,1,0:T(8,128)S(1)}, u32[]{:S(2)}) copy-start(f32[8,4,128,128]{3,2,1,0:T(8,128)S(1)} %multiply_add_fusion) | copy-start | bytes 6291460
  51.9 0.7 copy-start.7
  51.9 4.9 %copy-start.9 = (bf16[128]{0:T(256)(128)(2,1)S(1)}, bf16[128]{0:T(256)(128)(2,1)}, u32[]{:S(2)}) copy-start(bf16[128]{0:T(256)(128)(2,1)} %param.28) | copy-start | bytes 772
  51.9 11.7 %copy-start.6 = (bf16[512,128]{1,0:T(8,128)(2,1)S(1)}, bf16[512,128]{1,0:T(8,128)(2,1)}, u32[]{:S(2)}) copy-start(bf16[512,128]{1,0:T(8,128)(2,1)} %param.27) | copy-start | bytes 393220
  51.9 19.8 %copy-start.5 = (bf16[128,64]{0,1:T(8,128)(2,1)S(1)}, bf16[128,64]{0,1:T(8,128)(2,1)}, u32[]{:S(2)}) copy-start(bf16[128,64]{0,1:T(8,128)(2,1)} %param.16) | copy-start | bytes 49156
  52.0 42.0 %copy-start.3 = (bf16[1024,352]{0,1:T(8,128)(2,1)S(1)}, bf16[1024,352]{0,1:T(8,128)(2,1)}, u32[]{:S(2)}) copy-start(bf16[1024,352]{0,1:T(8,128)(2,1)} %param.29) | copy-start | bytes 2162692
  52.0 42.3 %copy-start.4 = (bf16[1024,352]{0,1:T(8,128)(2,1)S(1)}, bf16[1024,352]{0,1:T(8,128)(2,1)}, u32[]{:S(2)}) copy-start(bf16[1024,352]{0,1:T(8,128)(2,1)} %param.30) | copy-start | bytes 2162692
  53.3 10.3 %all-to-all-start.3 = ((bf16[16,8,512]{2,1,0:T(8,128)(2,1)}), bf16[16,8,512]{2,1,0:T(8,128)(2,1)S(1)}, u32[]{:S(2)}, u32[]{:S(2)}) async-start(bf16[16,8,512]{2,1,0:T(8,128)(2,1)} %broadcast_in_dim.14), calls=%async_computation.3 | async-start | bytes 262144 | tf_op jit(solution)/shard_map/all_to_all | solution.py:19
  72.4 9.8 %all-to-all-start.7 = ((bf16[16,128,1]{1,2,0:T(2,128)(2,1)}), bf16[16,128,1]{1,2,0:T(2,128)(2,1)S(1)}, u32[]{:S(2)}, u32[]{:S(2)}) async-start(bf16[16,128,1]{1,2,0:T(2,128)(2,1)} %broadcast_in_dim.17), calls=%async_computation.7 | async-start | bytes 16384 | tf_op jit(solution)/shard_map/all_to_all | solution.py:19
  82.9 11.0 %all-to-all-start.5 = ((bf16[16,128,64]{1,2,0:T(8,128)(2,1)}), bf16[16,128,64]{1,2,0:T(8,128)(2,1)S(1)}, u32[]{:S(2)}, u32[]{:S(2)}) async-start(bf16[16,128,64]{1,2,0:T(8,128)(2,1)} %broadcast_in_dim.15), calls=%async_computation.5 | async-start | bytes 524288 | tf_op jit(solution)/shard_map/all_to_all | solution.py:19
where the time goes:
time: 114 us; the launch traced here: 113 us
  blocking collectives  48.4 us (42%)
  starting transfers between devices  26.2 us (23%)
  waiting for transfers between devices  17.4 us (15%)
  matrix products  8.36 us (7%)
  local copies, waits for them, and re-layouts  7.64 us (7%)
  other arithmetic  4 us (4%)
    psum x2, blocking collectives, by_axis(): array = lax.psum(array, axis)  20.6 us
    all_to_all x2, blocking collectives, sum_at_owner(): lax.all_to_all(split_up(array, dim, devices), axis, 0, 0, tiled=True)  18.6 us
    all_to_all x5, starting transfers between devices, from_everyone(): return lax.all_to_all(copies, axis, split_axis=0, concat_axis=0, tiled=True)  18.3 us
    all_to_all x5, waiting for transfers between devices, from_everyone(): return lax.all_to_all(copies, axis, split_axis=0, concat_axis=0, tiled=True)  17.4 us
    all_to_all x1, starting transfers between devices, sum_at_owner(): lax.all_to_all(split_up(array, dim, devices), axis, 0, 0, tiled=True)  7.88 us
    dot_general x6, matrix products, local(): jnp.dot(row_block, weight, preferred_element_type=jnp.float32)  6.29 us
    all_to_all x1, blocking collectives, from_everyone(): return lax.all_to_all(copies, axis, split_axis=0, concat_axis=0, tiled=True)  6.28 us
    broadcast_in_dim x6, local copies, waits for them, and re-layouts, from_everyone(): copies = jnp.broadcast_to(array, (lax.axis_size(axis), *array.shape))  4 us
  transfers between devices with their start and end apart: 6, of which 3 were waited for; matrix products, arithmetic and copies ran while one was open for 9% of the time, Pallas kernels for 0%

commit v1 on v0

v1 whole, which is shorter than its diff:
```python
import jax
import jax.numpy as jnp
from jax import lax
from jax.sharding import Mesh
from jax.sharding import PartitionSpec as P

D = 2048
HEAD_DIM = 128
KV = ("kv_0", "kv_1")
KV_TP = ("kv_0", "kv_1", "tp")
DP_KV = ("dp", "kv_0", "kv_1")


norm_epsilon = 1e-06


def from_everyone(array, axis):
    copies = jnp.broadcast_to(array, (lax.axis_size(axis), *array.shape))
    return lax.all_to_all(copies, axis, split_axis=0, concat_axis=0, tiled=True)


def from_other_core(array):
    return lax.ppermute(array, "tp", [(0, 1), (1, 0)])


def two_halves(value):
    high = value.astype(jnp.bfloat16)
    low = (value - high.astype(jnp.float32)).astype(jnp.bfloat16)
    return high, low


def unit_rows(vector):
    return vector * lax.rsqrt(jnp.sum(vector * vector, axis=-1, keepdims=True) + norm_epsilon)


def mixer_core(
    query_lin, key_lin, value_lin, gate_lin, beta_lin, decay_lin, delta_state, decay_rate, head_gain
):
    seq_count = query_lin.shape[0]
    head_count = beta_lin.shape[1]
    shaped = lambda matrix: matrix.reshape(seq_count, head_count, HEAD_DIM)
    query = unit_rows(jax.nn.silu(shaped(query_lin))) * HEAD_DIM ** (-0.5)
    key_vec = unit_rows(jax.nn.silu(shaped(key_lin)))
    value_vec = jax.nn.silu(shaped(value_lin))
    write_rate = jax.nn.sigmoid(beta_lin)
    keep_rate = jnp.exp(-decay_rate[None, :] * jax.nn.softplus(decay_lin))
    recalled = jnp.einsum("bhkv,bhk->bhv", delta_state, key_vec)
    asked = jnp.einsum("bhkv,bhk->bhv", delta_state, query)
    correction = write_rate[..., None] * (value_vec - keep_rate[..., None] * recalled)
    overlap = jnp.sum(key_vec * query, axis=-1, keepdims=True)
    readout = keep_rate[..., None] * asked + overlap * correction
    readout = readout * lax.rsqrt(
        jnp.mean(readout * readout, axis=-1, keepdims=True) + norm_epsilon
    )
    readout = readout * head_gain * jax.nn.silu(shaped(gate_lin))
    next_state = (
        keep_rate[..., None, None] * delta_state + key_vec[..., :, None] * correction[..., None, :]
    )
    return (readout.reshape(seq_count, head_count * HEAD_DIM).astype(jnp.bfloat16), next_state)


def local(
    tokens,
    delta_state,
    gain_in,
    w_query,
    w_key,
    w_value,
    w_out_gate,
    w_beta,
    w_decay,
    decay_rate,
    head_gain,
    w_mix,
    gain_mid,
    w_gate,
    w_up,
    w_down,
):
    group_size = lax.axis_size(KV)
    core_pos = lax.axis_index("tp")
    on_first = core_pos == 0
    all_rows = tokens.shape[0]
    own_rows = all_rows // group_size
    feature_count = tokens.shape[1]
    head_count = w_query.shape[1] // HEAD_DIM
    width_dev = w_query.shape[1]
    token_float = tokens.astype(jnp.float32)
    other_tokens = from_other_core(tokens)
    whole_rows = jnp.concatenate(
        [
            jnp.where(on_first, tokens, other_tokens),
            jnp.where(on_first, other_tokens, tokens),
        ],
        axis=1,
    ).astype(jnp.float32)
    normed = (whole_rows * gain_in.astype(jnp.float32)).astype(jnp.bfloat16)
    squares = two_halves(jnp.sum(whole_rows * whole_rows, axis=1, keepdims=True))
    beta_cols = lax.dynamic_slice_in_dim(w_beta, core_pos * head_count, head_count, 1)
    decay_cols = lax.dynamic_slice_in_dim(w_decay, core_pos * head_count, head_count, 1)
    results = [
        jnp.dot(normed, weight, preferred_element_type=jnp.float32).astype(jnp.bfloat16)
        for weight in (w_query, w_key, w_value, w_out_gate, beta_cols, decay_cols)
    ]
    summand = jnp.concatenate([*results, *squares], axis=1)
    summand = summand.reshape(group_size, own_rows, summand.shape[1])
    pieces = lax.all_to_all(summand, KV, 0, 0, tiled=True)
    projected = jnp.sum(pieces.astype(jnp.float32), axis=0)
    gates_at = 4 * width_dev
    squares_at = gates_at + 2 * head_count
    square_total = projected[:, squares_at : squares_at + 1] + projected[:, squares_at + 1 :]
    row_scale = lax.rsqrt(square_total / D + norm_epsilon)
    projected = projected * row_scale
    mixed, next_state = mixer_core(
        projected[:, :width_dev],
        projected[:, width_dev : 2 * width_dev],
        projected[:, 2 * width_dev : 3 * width_dev],
        projected[:, 3 * width_dev : 4 * width_dev],
        projected[:, gates_at : gates_at + head_count],
        projected[:, gates_at + head_count : squares_at],
        delta_state,
        decay_rate,
        head_gain,
    )
    mixed_rows = from_everyone(mixed, KV).reshape(all_rows, width_dev)
    attn_part = jnp.dot(mixed_rows, w_mix, preferred_element_type=jnp.float32)
    own_part = lax.dynamic_slice_in_dim(attn_part, core_pos * feature_count, feature_count, 1)
    sent_part = lax.dynamic_slice_in_dim(
        attn_part, (1 - core_pos) * feature_count, feature_count, 1
    ).astype(jnp.bfloat16)
    attn = own_part + from_other_core(sent_part).astype(jnp.float32)
    middle_float = (token_float + attn).astype(jnp.bfloat16).astype(jnp.float32)
    mid_squares = two_halves(jnp.sum(middle_float * middle_float, axis=1, keepdims=True))
    gain_own = lax.dynamic_slice_in_dim(gain_mid, core_pos * feature_count, feature_count, 0)
    normed_own = (middle_float * gain_own.astype(jnp.float32)).astype(jnp.bfloat16)
    sent = jnp.concatenate([normed_own, *mid_squares], axis=1)
    received = from_everyone(sent, KV)
    normed_half = jnp.moveaxis(received[:, :, :feature_count], 0, 1).reshape(
        all_rows, group_size * feature_count
    )
    half_total = jnp.sum(received[:, :, feature_count:].astype(jnp.float32), axis=(0, 2))
    hidden_dev = w_gate.shape[1]
    summand = jnp.concatenate(
        [
            jnp.dot(normed_half, w_gate, preferred_element_type=jnp.float32),
            jnp.dot(normed_half, w_up, preferred_element_type=jnp.float32),
        ],
        axis=1,
    )
    gate_up = summand + from_other_core(summand.astype(jnp.bfloat16)).astype(jnp.float32)
    mid_total = half_total + from_other_core(half_total)
    mid_scale = lax.rsqrt(mid_total / D + norm_epsilon)
    gate_up = gate_up * mid_scale[:, None]
    activated = (jax.nn.silu(gate_up[:, :hidden_dev]) * gate_up[:, hidden_dev:]).astype(
        jnp.bfloat16
    )
    down_local = jnp.dot(activated, w_down, preferred_element_type=jnp.float32)
    tiles = down_local.astype(jnp.bfloat16).reshape(all_rows, group_size, feature_count)
    pieces = lax.all_to_all(jnp.moveaxis(tiles, 1, 0), KV, 0, 0, tiled=True)
    down_part = jnp.sum(pieces.astype(jnp.float32), axis=0)
    layer_out = (middle_float + down_part).astype(jnp.bfloat16)
    return (layer_out, next_state)


def solution(mesh):
    split = Mesh(
        mesh.devices.reshape(mesh.shape["dp"], 4, 4, mesh.shape["tp"]), ("dp", "kv_0", "kv_1", "tp")
    )
    in_specs = (
        P("dp", KV_TP),
        P(DP_KV, "tp", None, None),
        P(KV),
        P(KV, "tp"),
        P(KV, "tp"),
        P(KV, "tp"),
        P(KV, "tp"),
        P(KV, None),
        P(KV, None),
        P("tp"),
        P(),
        P("tp", KV),
        P(KV),
        P("tp", KV),
        P("tp", KV),
        P(KV, "tp"),
    )
    out_specs = (P("dp", KV_TP), P(DP_KV, "tp", None, None))
    return jax.shard_map(local, mesh=split, in_specs=in_specs, out_specs=out_specs, check_vma=False)
```

time: 114 us -> 82.9 us (0.73)
  blocking collectives: 48.4 us -> 0 us
  waiting for transfers between devices: 17.4 us -> 35.9 us
  local copies, waits for them, and re-layouts: 7.64 us -> 4.22 us
  matrix products: 8.36 us -> 10.9 us
  starting transfers between devices: 26.2 us -> 24.2 us
  other arithmetic: 4 us -> 5.95 us
    all_to_all x3 -> x0, blocking collectives: 24.9 us -> none  [the longest x2 18.6 us: sum_at_owner(): lax.all_to_all(split_up(array, dim, devices), axis, 0, 0, tiled=True)]
    psum x2 -> x0, blocking collectives: 20.6 us -> none  [by_axis(): array = lax.psum(array, axis)]
    all_to_all x1 -> x2, waiting for transfers between devices: 0.01 us -> 17.9 us  [the longest x1 11.1 us: local(): pieces = lax.all_to_all(summand, KV, 0, 0, tiled=True)]
    all_to_all x5 -> x2, starting transfers between devices: 18.3 us -> 7.05 us  [from_everyone(): return lax.all_to_all(copies, axis, split_axis=0, concat_axis=0, tiled=True)]
    ppermute x0 -> x4, starting transfers between devices: none -> 5.79 us  [from_other_core(): return lax.ppermute(array, 'tp', [(0, 1), (1, 0)])]
    all_to_all x1 -> x2, starting transfers between devices: 7.88 us -> 11.4 us  [the longest x1 7.88 us: local(): pieces = lax.all_to_all(summand, KV, 0, 0, tiled=True)]
    all_gather x1 -> x0, blocking collectives: 2.95 us -> none  [total_of_pieces(): return lax.all_gather(array, axis).sum(0)]
    broadcast_in_dim x6 -> x2, local copies, waits for them, and re-layouts: 4 us -> 1.43 us  [from_everyone(): copies = jnp.broadcast_to(array, (lax.axis_size(axis), *array.shape))]
  transfers between devices with their start and end apart: 6 -> 8, of which waited for: 3 -> 7; matrix products, arithmetic and copies ran while one was open for 9% -> 7% of each run, Pallas kernels for 0% -> 0%
where the time goes in v1:
time: 82.9 us; the launch traced here: 82.2 us
  waiting for transfers between devices  35.9 us (43%)
  starting transfers between devices  24.2 us (29%)
  matrix products  10.9 us (13%)
  other arithmetic  5.95 us (7%)
  local copies, waits for them, and re-layouts  4.22 us (5%)
  between operations  0.92 us (1%)
    all_to_all x2, waiting for transfers between devices, from_everyone(): return lax.all_to_all(copies, axis, split_axis=0, concat_axis=0, tiled=True)  15.5 us
    all_to_all x1, waiting for transfers between devices, local(): pieces = lax.all_to_all(summand, KV, 0, 0, tiled=True)  11.1 us
    all_to_all x1, starting transfers between devices, local(): pieces = lax.all_to_all(summand, KV, 0, 0, tiled=True)  7.88 us
    all_to_all x2, starting transfers between devices, from_everyone(): return lax.all_to_all(copies, axis, split_axis=0, concat_axis=0, tiled=True)  7.05 us
    all_to_all x1, waiting for transfers between devices, local(): pieces = lax.all_to_all(jnp.moveaxis(tiles, 1, 0), KV, 0, 0, tiled=True)  6.76 us
    dot_general x6, matrix products, local(): jnp.dot(normed, weight, preferred_element_type=jnp.float32)  6.63 us
    ppermute x4, starting transfers between devices, from_other_core(): return lax.ppermute(array, 'tp', [(0, 1), (1, 0)])  5.79 us
    all_to_all x1, starting transfers between devices, local(): pieces = lax.all_to_all(jnp.moveaxis(tiles, 1, 0), KV, 0, 0, tiled=True)  3.53 us
  transfers between devices with their start and end apart: 8, of which 7 were waited for; matrix products, arithmetic and copies ran while one was open for 7% of the time, Pallas kernels for 0%

profile of v1, /device:TPU:1, one launch (start us, length us, event | category | flops | bytes accessed | tf_op | source)
XLA Modules:
  0.0 82.2 jit_solution(3088590159829286306)
XLA Ops:
  0.7 1.5 %collective-permute-start = (bf16[128,64]{0,1:T(8,128)(2,1)}, bf16[128,64]{0,1:T(8,128)(2,1)S(1)}, u32[]{:S(2)}, u32[]{:S(2)}) collective-permute-start(bf16[128,64]{0,1:T(8,128)(2,1)} %param.16), channel_id=1, source_target_pairs={{0,1},{1,0},{2,3},{3,2},{4,5},{5,4},{6,7},{7,6},{8,9},{9,8},{10,11... | collective-permute-start | bytes 49160 | tf_op jit(solution)/shard_map/ppermute | solution.py:23
  3.9 0.9 %convolution_convert_fusion.6 = bf16[128,4]{0,1:T(4,128)(2,1)S(1)} fusion(bf16[128,8]{0,1:T(8,128)(2,1)} %param.23, s32[]{:T(128)S(6)} %select_n.30, f32[128]{0:T(128)S(1)} %convert_element_type.158, bf16[128,64]{0,1:T(8,128)(2,1)S(1)} %get-tuple-element.11, bf16[128,64]{0,1:T(8,128)(2,1)S(1)} %get-tuple-element.10), kind=kOutput, calls=%fused_computation.15 | convolution fusion | flops 229888 | bytes 35332 | tf_op jit(solution)/shard_map/dot_general | solution.py:102
  4.8 0.9 %convolution_convert_fusion.5 = bf16[128,4]{0,1:T(4,128)(2,1)S(1)} fusion(bf16[128,8]{0,1:T(8,128)(2,1)} %param.24, s32[]{:T(128)S(6)} %select_n.30, f32[128]{0:T(128)S(1)} %convert_element_type.158, bf16[128,64]{0,1:T(8,128)(2,1)S(1)} %get-tuple-element.11, bf16[128,64]{0,1:T(8,128)(2,1)S(1)} %get-tuple-element.10), kind=kOutput, calls=%fused_computation.14 | convolution fusion | flops 229888 | bytes 35332 | tf_op jit(solution)/shard_map/dot_general | solution.py:102
  6.4 1.2 %fusion.2 = bf16[16,8,512]{2,1,0:T(8,128)(2,1)S(1)} fusion(bf16[128,512]{1,0:T(8,128)(2,1)} %param.20, f32[128]{0:T(128)S(1)} %convert_element_type.158, bf16[128,64]{0,1:T(8,128)(2,1)S(1)} %get-tuple-element.11, bf16[128,64]{0,1:T(8,128)(2,1)S(1)} %get-tuple-element.10), kind=kOutput, calls=%fused_computation.8 | convolution fusion | flops 16941056 | bytes 295424 | tf_op jit(solution)/shard_map/dot_general | solution.py:102
  7.6 1.3 %fusion.3 = bf16[16,8,512]{2,1,0:T(8,128)(2,1)S(1)} fusion(bf16[128,512]{1,0:T(8,128)(2,1)} %param.21, f32[128]{0:T(128)S(1)} %convert_element_type.158, bf16[128,64]{0,1:T(8,128)(2,1)S(1)} %get-tuple-element.11, bf16[128,64]{0,1:T(8,128)(2,1)S(1)} %get-tuple-element.10), kind=kOutput, calls=%fused_computation.9 | convolution fusion | flops 16941056 | bytes 295424 | tf_op jit(solution)/shard_map/dot_general | solution.py:102
  9.0 1.2 %fusion.4 = bf16[16,8,512]{2,1,0:T(8,128)(2,1)S(1)} fusion(bf16[128,512]{1,0:T(8,128)(2,1)} %param.22, f32[128]{0:T(128)S(1)} %convert_element_type.158, bf16[128,64]{0,1:T(8,128)(2,1)S(1)} %get-tuple-element.11, bf16[128,64]{0,1:T(8,128)(2,1)S(1)} %get-tuple-element.10), kind=kOutput, calls=%fused_computation.10 | convolution fusion | flops 16941056 | bytes 295424 | tf_op jit(solution)/shard_map/dot_general | solution.py:102
  10.2 1.2 %fusion.1 = bf16[16,8,512]{2,1,0:T(8,128)(2,1)S(1)} fusion(bf16[128,512]{1,0:T(8,128)(2,1)} %param.19, f32[128]{0:T(128)S(1)} %convert_element_type.158, bf16[128,64]{0,1:T(8,128)(2,1)S(1)} %get-tuple-element.11, bf16[128,64]{0,1:T(8,128)(2,1)S(1)} %get-tuple-element.10), kind=kOutput, calls=%fused_computation.7 | convolution fusion | flops 16941056 | bytes 295424 | tf_op jit(solution)/shard_map/dot_general | solution.py:102
  11.4 1.0 %concatenate.32 = bf16[16,8,2058]{2,1,0:T(8,128)(2,1)} concatenate(bf16[16,8,512]{2,1,0:T(8,128)(2,1)S(1)} %fusion.1, bf16[16,8,512]{2,1,0:T(8,128)(2,1)S(1)} %fusion.2, bf16[16,8,512]{2,1,0:T(8,128)(2,1)S(1)} %fusion.3, bf16[16,8,512]{2,1,0:T(8,128)(2,1)S(1)} %fusion.4, bf16[16,8,4]{2,1,0:T(8,128)(2,1)S(1)} %bitcast.92, bf16[16,8,4]{2,1,0:T(8,128)(2,1)S(1)} %bitcast.91, ...), dimensions={2} | concatenate | bytes 1053696 | tf_op jit(solution)/shard_map/concatenate | solution.py:105
  12.3 7.9 %all-to-all-start = ((bf16[16,8,2058]{2,1,0:T(8,128)(2,1)}), bf16[16,8,2058]{2,1,0:T(8,128)(2,1)S(1)}, u32[]{:S(2)}, u32[]{:S(2)}) async-start(bf16[16,8,2058]{2,1,0:T(8,128)(2,1)} %concatenate.32), calls=%async_computation | async-start | bytes 1114112 | tf_op jit(solution)/shard_map/all_to_all | solution.py:107
  20.2 11.1 %all-to-all-done = bf16[16,8,2058]{2,1,0:T(8,128)(2,1)S(1)} async-done(((bf16[16,8,2058]{2,1,0:T(8,128)(2,1)}), bf16[16,8,2058]{2,1,0:T(8,128)(2,1)S(1)}, u32[]{:S(2)}, u32[]{:S(2)}) %all-to-all-start) | async-done | bytes 526880 | tf_op jit(solution)/shard_map/all_to_all | solution.py:107
  33.2 0.9 %multiply_reduce_fusion = (f32[8,4]{0,1:T(4,128)S(1)}, f32[8,4,128]{2,0,1:T(8,128)S(1)}) fusion(f32[8,4,128]{2,0,1:T(8,128)S(1)} %fusion.19, f32[8,4,128]{2,0,1:T(8,128)S(1)} %broadcast_multiply_fusion.1, f32[8,4]{0,1:T(4,128)S(1)} %get-tuple-element.15, f32[8,2058]{1,0:T(8,128)S(1)} %broadcast_multiply_fusion, f32[8,4,1,128]{3,2,1,0:T(1,128)S(1)} %fusion.22, ...), kind=kOutput, calls=%fused_computation.54 | output fusion | flops 49279 | bytes 86144 | tf_op jit(solution)/shard_map/mul | solution.py:51
  34.9 3.5 %all-to-all-start.1 = ((bf16[16,8,512]{2,1,0:T(8,128)(2,1)}), bf16[16,8,512]{2,1,0:T(8,128)(2,1)S(1)}, u32[]{:S(2)}, u32[]{:S(2)}) async-start(bf16[16,8,512]{2,1,0:T(8,128)(2,1)} %broadcast_in_dim.4), calls=%async_computation.1 | async-start | bytes 262144 | tf_op jit(solution)/shard_map/all_to_all | solution.py:19
  38.4 6.8 %all-to-all-done.1 = bf16[16,8,512]{2,1,0:T(8,128)(2,1)S(1)} async-done(((bf16[16,8,512]{2,1,0:T(8,128)(2,1)}), bf16[16,8,512]{2,1,0:T(8,128)(2,1)S(1)}, u32[]{:S(2)}, u32[]{:S(2)}) %all-to-all-start.1) | async-done | bytes 131104 | tf_op jit(solution)/shard_map/all_to_all | solution.py:19
  45.4 3.0 %collective-permute-start.1 = (bf16[128,64]{0,1:T(8,128)(2,1)S(1)}, bf16[128,64]{0,1:T(8,128)(2,1)S(1)}, u32[]{:S(2)}, u32[]{:S(2)}) collective-permute-start(bf16[128,64]{0,1:T(8,128)(2,1)S(1)} %dynamic-slice_convert_fusion), channel_id=1, source_target_pairs={{0,1},{1,0},{2,3},{3,2},{4,5},{5,4},{6,7},{7,6},{8,9},{9,8},{10,11... | collective-permute-start | bytes 49160 | tf_op jit(solution)/shard_map/ppermute | solution.py:23
  50.1 3.5 %all-to-all-start.2 = ((bf16[16,128,66]{1,2,0:T(8,128)(2,1)}), bf16[16,128,66]{1,2,0:T(8,128)(2,1)S(1)}, u32[]{:S(2)}, u32[]{:S(2)}) async-start(bf16[16,128,66]{1,2,0:T(8,128)(2,1)} %broadcast_in_dim.5), calls=%async_computation.2 | async-start | bytes 589824 | tf_op jit(solution)/shard_map/all_to_all | solution.py:19
  53.7 8.7 %all-to-all-done.2 = bf16[16,128,66]{1,2,0:T(8,128)(2,1)S(1)} async-done(((bf16[16,128,66]{1,2,0:T(8,128)(2,1)}), bf16[16,128,66]{1,2,0:T(8,128)(2,1)S(1)}, u32[]{:S(2)}, u32[]{:S(2)}) %all-to-all-start.2) | async-done | bytes 270368 | tf_op jit(solution)/shard_map/all_to_all | solution.py:19
  62.5 1.3 %collective-permute-start.3 = (f32[128]{0:T(128)S(1)}, f32[128]{0:T(128)S(1)}, u32[]{:S(2)}, u32[]{:S(2)}) collective-permute-start(f32[128]{0:T(128)S(1)} %convert_reduce_fusion.2), channel_id=1, source_target_pairs={{0,1},{1,0},{2,3},{3,2},{4,5},{5,4},{6,7},{7,6},{8,9},{9,8},{10,11... | collective-permute-start | bytes 1544 | tf_op jit(solution)/shard_map/ppermute | solution.py:23
  63.8 1.5 %fusion.52 = f32[128,352]{0,1:T(8,128)S(1)} fusion(bf16[1024,352]{0,1:T(8,128)(2,1)} %param.29, bf16[128,1024]{0,1:T(8,128)(2,1)S(1)} %bitcast.89), kind=kOutput, calls=%fused_computation.95 | convolution fusion | flops 92274688 | bytes 1163264 | tf_op jit(solution)/shard_map/dot_general | solution.py:145
  65.2 1.5 %fusion.53 = f32[128,352]{0,1:T(8,128)S(1)} fusion(bf16[1024,352]{0,1:T(8,128)(2,1)} %param.30, bf16[128,1024]{0,1:T(8,128)(2,1)S(1)} %bitcast.90), kind=kOutput, calls=%fused_computation.96 | convolution fusion | flops 92274688 | bytes 1163264 | tf_op jit(solution)/shard_map/dot_general | solution.py:146
  66.8 1.4 %collective-permute-done.2 = bf16[128,704]{0,1:T(8,128)(2,1)S(1)} collective-permute-done((bf16[128,704]{0,1:T(8,128)(2,1)S(1)}, bf16[128,704]{0,1:T(8,128)(2,1)S(1)}, u32[]{:S(2)}, u32[]{:S(2)}) %collective-permute-start.2) | collective-permute-done | bytes 180256 | tf_op jit(solution)/shard_map/ppermute | solution.py:23
  68.6 0.8 %copy.68 = bf16[128,1024]{0,1:T(8,128)(2,1)} copy(bf16[128,1024]{1,0:T(8,128)(2,1)S(1)} %convolution_convert_fusion) | data formatting | bytes 524288 | tf_op jit(solution)/shard_map/convert_element_type | solution.py:158
  69.5 3.5 %all-to-all-start.3 = ((bf16[16,128,64]{1,2,0:T(8,128)(2,1)}), bf16[16,128,64]{1,2,0:T(8,128)(2,1)S(1)}, u32[]{:S(2)}, u32[]{:S(2)}) async-start(bf16[16,128,64]{1,2,0:T(8,128)(2,1)} %bitcast.21), calls=%async_computation.3 | async-start | bytes 524288 | tf_op jit(solution)/shard_map/all_to_all | solution.py:159
  73.0 1.7 %multiply_add_fusion = f32[8,4,128,128]{3,2,1,0:T(8,128)} fusion(f32[8,4,128,128]{3,2,1,0:T(8,128)S(1)} %copy-done.1, f32[8,4,128]{2,1,0:T(4,128)S(1)} %copy.70, f32[8,4,128]{2,1,0:T(4,128)S(1)} %copy.69, f32[8,4]{1,0:T(8,128)S(1)} %get-tuple-element.8), kind=kLoop, calls=%fused_computation.1 | loop fusion | flops 1572864 | bytes 4227200 | tf_op jit(solution)/shard_map/add | solution.py:57
  74.7 6.8 %all-to-all-done.3 = bf16[16,128,64]{1,2,0:T(8,128)(2,1)S(1)} async-done(((bf16[16,128,64]{1,2,0:T(8,128)(2,1)}), bf16[16,128,64]{1,2,0:T(8,128)(2,1)S(1)}, u32[]{:S(2)}, u32[]{:S(2)}) %all-to-all-start.3) | async-done | bytes 262176 | tf_op jit(solution)/shard_map/all_to_all | solution.py:159
  (65 shorter events, 8.3 us)
Async XLA Ops:
  0.6 67.6 %copy-start = (bf16[352,1024]{1,0:T(8,128)(2,1)S(1)}, bf16[352,1024]{1,0:T(8,128)(2,1)}, u32[]{:S(2)}) copy-start(bf16[352,1024]{1,0:T(8,128)(2,1)} %param.31) | copy-start | bytes 2162692
  0.6 19.6 %copy-start.5 = (f32[4]{0:T(128)S(1)}, f32[4]{0:T(128)}, u32[]{:S(2)}) copy-start(f32[4]{0:T(128)} %param.25) | copy-start | bytes 52
  0.7 2.5 %collective-permute-start = (bf16[128,64]{0,1:T(8,128)(2,1)}, bf16[128,64]{0,1:T(8,128)(2,1)S(1)}, u32[]{:S(2)}, u32[]{:S(2)}) collective-permute-start(bf16[128,64]{0,1:T(8,128)(2,1)} %param.16), channel_id=1, source_target_pairs={{0,1},{1,0},{2,3},{3,2},{4,5},{5,4},{6,7},{7,6},{8,9},{9,8},{10,11... | collective-permute-start | bytes 49160 | tf_op jit(solution)/shard_map/ppermute | solution.py:23
  7.6 24.7 %copy-start.1 = (f32[8,4,128,128]{3,2,1,0:T(8,128)S(1)}, f32[8,4,128,128]{3,2,1,0:T(8,128)}, u32[]{:S(2)}) copy-start(f32[8,4,128,128]{3,2,1,0:T(8,128)} %param.17) | copy-start | bytes 6291460
  12.3 19.0 %all-to-all-start = ((bf16[16,8,2058]{2,1,0:T(8,128)(2,1)}), bf16[16,8,2058]{2,1,0:T(8,128)(2,1)S(1)}, u32[]{:S(2)}, u32[]{:S(2)}) async-start(bf16[16,8,2058]{2,1,0:T(8,128)(2,1)} %concatenate.32), calls=%async_computation | async-start | bytes 1114112 | tf_op jit(solution)/shard_map/all_to_all | solution.py:107
  32.3 1.8 %copy-start.4 = (f32[128]{0:T(128)S(1)}, f32[128]{0:T(128)}, u32[]{:S(2)}) copy-start(f32[128]{0:T(128)} %param.26) | copy-start | bytes 1540
  32.3 12.9 %copy-start.2 = (bf16[512,128]{1,0:T(8,128)(2,1)S(1)}, bf16[512,128]{1,0:T(8,128)(2,1)}, u32[]{:S(2)}) copy-start(bf16[512,128]{1,0:T(8,128)(2,1)} %param.27) | copy-start | bytes 393220
  32.7 15.7 %copy-start.6 = (bf16[128]{0:T(256)(128)(2,1)S(1)}, bf16[128]{0:T(256)(128)(2,1)}, u32[]{:S(2)}) copy-start(bf16[128]{0:T(256)(128)(2,1)} %param.28) | copy-start | bytes 772
  32.7 16.5 %copy-start.3 = (bf16[128,64]{0,1:T(8,128)(2,1)S(1)}, bf16[128,64]{0,1:T(8,128)(2,1)}, u32[]{:S(2)}) copy-start(bf16[128,64]{0,1:T(8,128)(2,1)} %param.16) | copy-start | bytes 49156
  34.9 10.3 %all-to-all-start.1 = ((bf16[16,8,512]{2,1,0:T(8,128)(2,1)}), bf16[16,8,512]{2,1,0:T(8,128)(2,1)S(1)}, u32[]{:S(2)}, u32[]{:S(2)}) async-start(bf16[16,8,512]{2,1,0:T(8,128)(2,1)} %broadcast_in_dim.4), calls=%async_computation.1 | async-start | bytes 262144 | tf_op jit(solution)/shard_map/all_to_all | solution.py:19
  45.4 3.8 %collective-permute-start.1 = (bf16[128,64]{0,1:T(8,128)(2,1)S(1)}, bf16[128,64]{0,1:T(8,128)(2,1)S(1)}, u32[]{:S(2)}, u32[]{:S(2)}) collective-permute-start(bf16[128,64]{0,1:T(8,128)(2,1)S(1)} %dynamic-slice_convert_fusion), channel_id=1, source_target_pairs={{0,1},{1,0},{2,3},{3,2},{4,5},{5,4},{6,7},{7,6},{8,9},{9,8},{10,11... | collective-permute-start | bytes 49160 | tf_op jit(solution)/shard_map/ppermute | solution.py:23
  50.1 12.3 %all-to-all-start.2 = ((bf16[16,128,66]{1,2,0:T(8,128)(2,1)}), bf16[16,128,66]{1,2,0:T(8,128)(2,1)S(1)}, u32[]{:S(2)}, u32[]{:S(2)}) async-start(bf16[16,128,66]{1,2,0:T(8,128)(2,1)} %broadcast_in_dim.5), calls=%async_computation.2 | async-start | bytes 589824 | tf_op jit(solution)/shard_map/all_to_all | solution.py:19
  62.5 4.4 %collective-permute-start.3 = (f32[128]{0:T(128)S(1)}, f32[128]{0:T(128)S(1)}, u32[]{:S(2)}, u32[]{:S(2)}) collective-permute-start(f32[128]{0:T(128)S(1)} %convert_reduce_fusion.2), channel_id=1, source_target_pairs={{0,1},{1,0},{2,3},{3,2},{4,5},{5,4},{6,7},{7,6},{8,9},{9,8},{10,11... | collective-permute-start | bytes 1544 | tf_op jit(solution)/shard_map/ppermute | solution.py:23
  66.7 1.5 %collective-permute-start.2 = (bf16[128,704]{0,1:T(8,128)(2,1)S(1)}, bf16[128,704]{0,1:T(8,128)(2,1)S(1)}, u32[]{:S(2)}, u32[]{:S(2)}) collective-permute-start(bf16[128,704]{0,1:T(8,128)(2,1)S(1)} %fusion.7), channel_id=1, source_target_pairs={{0,1},{1,0},{2,3},{3,2},{4,5},{5,4},{6,7},{7,6},{8,9},{9,8},{10,11... | collective-permute-start | bytes 540680 | tf_op jit(solution)/shard_map/ppermute | solution.py:23
  69.5 12.0 %all-to-all-start.3 = ((bf16[16,128,64]{1,2,0:T(8,128)(2,1)}), bf16[16,128,64]{1,2,0:T(8,128)(2,1)S(1)}, u32[]{:S(2)}, u32[]{:S(2)}) async-start(bf16[16,128,64]{1,2,0:T(8,128)(2,1)} %bitcast.21), calls=%async_computation.3 | async-start | bytes 524288 | tf_op jit(solution)/shard_map/all_to_all | solution.py:159

commit v2 on v1

v2 whole, which is shorter than its diff:
```python
import jax
import jax.numpy as jnp
from jax import lax
from jax.experimental import pallas as pl
from jax.experimental.pallas import tpu as pltpu
from jax.sharding import Mesh
from jax.sharding import PartitionSpec as P

D = 2048
HEAD_DIM = 128
KV = ("kv_0", "kv_1")
KV_TP = ("kv_0", "kv_1", "tp")
DP_KV = ("dp", "kv_0", "kv_1")

norm_epsilon = 1e-06
bf16 = jnp.bfloat16
f32 = jnp.float32

GROUP = 16
ROWS = 128
OWN = ROWS // GROUP
FEAT = 64
HEADS_DEV = 4
WIDTH_DEV = HEADS_DEV * HEAD_DIM
PIECE = 4 * WIDTH_DEV + 128
SQUARE_AT = 4 * WIDTH_DEV + 2 * HEADS_DEV
TALL = FEAT + 8
HIDDEN = 352
BOTH = 2 * HIDDEN

TN = (((0,), (0,)), ((), ()))
NT = (((1,), (1,)), ((), ()))


def in_vmem():
    return pl.BlockSpec(memory_space=pltpu.VMEM)


def anywhere():
    return pl.BlockSpec(memory_space=pl.ANY)


def shape(lengths, dtype):
    return jax.ShapeDtypeStruct(lengths, dtype)


def kernel(body, name, outs, in_specs, limit=12):
    single = not isinstance(outs, (list, tuple))
    return pl.pallas_call(
        body,
        out_shape=outs,
        in_specs=in_specs,
        out_specs=in_vmem() if single else [in_vmem() for _ in outs],
        name=name,
        compiler_params=pltpu.CompilerParams(vmem_limit_bytes=limit * 1024 * 1024),
    )


def silu(value):
    return value / (1.0 + jnp.exp(-value))


def high_low(value):
    high = value.astype(bf16).astype(f32)
    return high, value - high


def dot(left, right, dims=(((1,), (0,)), ((), ()))):
    return lax.dot_general(left, right, dims, preferred_element_type=f32)


def project(own_ref, other_ref, gain_ref, wq_ref, wk_ref, wv_ref, wg_ref, wb_ref, wd_ref, out_ref):
    on_first = lax.axis_index("tp") == 0
    own = own_ref[...].astype(f32)
    other = other_ref[...].astype(f32)
    rows = jnp.concatenate(
        [jnp.where(on_first, own, other), jnp.where(on_first, other, own)], axis=0
    ).T
    high, low = high_low(jnp.sum(rows * rows, axis=1, keepdims=True))
    normed = (rows * gain_ref[...].astype(f32)).astype(bf16)
    for at, ref in enumerate((wq_ref, wk_ref, wv_ref, wg_ref)):
        out_ref[:, at * WIDTH_DEV : (at + 1) * WIDTH_DEV] = dot(normed, ref[...]).astype(bf16)
    beta = wb_ref[...].astype(f32)
    decay = wd_ref[...].astype(f32)
    small = jnp.concatenate(
        [
            jnp.where(on_first, beta[:HEADS_DEV], beta[HEADS_DEV:]),
            jnp.where(on_first, decay[:HEADS_DEV], decay[HEADS_DEV:]),
            jnp.zeros((128 - 2 * HEADS_DEV, 128), f32),
        ],
        axis=0,
    ).astype(bf16)
    extra = dot(normed, small, NT)
    lane = lax.broadcasted_iota(jnp.int32, extra.shape, 1)
    extra = jnp.where(lane == 2 * HEADS_DEV, high, extra)
    extra = jnp.where(lane == 2 * HEADS_DEV + 1, low, extra)
    out_ref[:, 4 * WIDTH_DEV :] = extra.astype(bf16)


def mixer(pieces_ref, state_ref, rate_ref, head_gain_ref, mixed_ref, key_ref, correct_ref, keep_ref):
    def total(first, last):
        parts = [pieces_ref[OWN * s : OWN * (s + 1), first:last].astype(f32) for s in range(GROUP)]
        while len(parts) > 1:
            parts = [a + b for a, b in zip(parts[::2], parts[1::2])]
        return parts[0]

    small = total(4 * WIDTH_DEV, PIECE)
    square = 2 * HEADS_DEV
    row_scale = lax.rsqrt(
        (small[:, square : square + 1] + small[:, square + 1 : square + 2]) / D + norm_epsilon
    )
    small = small * row_scale
    row = lax.broadcasted_iota(jnp.int32, (OWN, HEAD_DIM), 0)
    lane = lax.broadcasted_iota(jnp.int32, (OWN, HEAD_DIM), 1)
    keeps = jnp.zeros((OWN, HEAD_DIM), f32)

    def unit(vector):
        return vector * lax.rsqrt(jnp.sum(vector * vector, axis=1, keepdims=True) + norm_epsilon)

    for h in range(HEADS_DEV):
        at = h * HEAD_DIM
        query_lin, key_lin, value_lin, gate_lin = (
            total(part * WIDTH_DEV + at, part * WIDTH_DEV + at + HEAD_DIM) * row_scale
            for part in range(4)
        )
        query = unit(silu(query_lin)) * HEAD_DIM ** (-0.5)
        key = unit(silu(key_lin))
        write_rate = 1.0 / (1.0 + jnp.exp(-small[:, h : h + 1]))
        decay = small[:, HEADS_DEV + h : HEADS_DEV + h + 1]
        softplus = jnp.maximum(decay, 0.0) + jnp.log1p(jnp.exp(-jnp.abs(decay)))
        keep = jnp.exp(-rate_ref[:, h : h + 1] * softplus)
        pair = jnp.concatenate([key, query], axis=0).astype(bf16)
        recalled = jnp.zeros((OWN, HEAD_DIM), f32)
        asked = jnp.zeros((OWN, HEAD_DIM), f32)
        for b in range(OWN):
            both = dot(pair, state_ref[b, h].astype(bf16))
            recalled = jnp.where(row == b, both[:OWN], recalled)
            asked = jnp.where(row == b, both[OWN:], asked)
        correction = write_rate * (silu(value_lin) - keep * recalled)
        readout = keep * asked + jnp.sum(key * query, axis=1, keepdims=True) * correction
        readout = readout * lax.rsqrt(
            jnp.mean(readout * readout, axis=1, keepdims=True) + norm_epsilon
        )
        mixed = (readout * head_gain_ref[...] * silu(gate_lin)).astype(bf16)
        for s in range(GROUP):
            mixed_ref[OWN * s : OWN * (s + 1), at : at + HEAD_DIM] = mixed
        key_ref[:, at : at + HEAD_DIM] = key
        correct_ref[:, at : at + HEAD_DIM] = correction
        keeps = jnp.where(lane == h, keep, keeps)
    keep_ref[...] = keeps


def update(state_ref, key_ref, correct_ref, keep_ref, after_ref, next_ref):
    del after_ref
    b = pl.program_id(0)
    pick = lax.broadcasted_iota(jnp.int32, (OWN, WIDTH_DEV), 0) == b
    key = jnp.sum(jnp.where(pick, key_ref[...], 0.0), axis=0, keepdims=True)
    correction = jnp.sum(jnp.where(pick, correct_ref[...], 0.0), axis=0, keepdims=True)
    keep = jnp.sum(jnp.where(pick[:, :HEAD_DIM], keep_ref[...], 0.0), axis=0, keepdims=True)
    for h in range(HEADS_DEV):
        at = h * HEAD_DIM
        key_column = jnp.broadcast_to(key[:, at : at + HEAD_DIM], (HEAD_DIM, HEAD_DIM)).T
        next_ref[0, h] = (
            keep[:, h : h + 1] * state_ref[0, h] + key_column * correction[:, at : at + HEAD_DIM]
        )


def mix(mixed_ref, w_ref, own_ref, sent_ref):
    on_first = lax.axis_index("tp") == 0
    part = dot(mixed_ref[...], w_ref[...]).T
    own_ref[...] = jnp.where(on_first, part[:FEAT], part[FEAT:])
    sent_ref[...] = jnp.where(on_first, part[FEAT:], part[:FEAT]).astype(bf16)


def middle_rows(tokens_ref, own_ref, other_ref, gain_ref, middle_ref, sent_ref):
    on_first = lax.axis_index("tp") == 0
    gains = jnp.broadcast_to(gain_ref[...].astype(f32), (128, 128)).T
    gain = jnp.where(on_first, gains[:FEAT], gains[FEAT:])
    middle = tokens_ref[...].astype(f32) + (own_ref[...] + other_ref[...].astype(f32))
    middle_ref[...] = middle.astype(bf16)
    middle = middle.astype(bf16).astype(f32)
    normed = (middle * gain).astype(bf16)
    high, low = high_low(jnp.sum(middle * middle, axis=0, keepdims=True))
    squares = jnp.concatenate([high, low, jnp.zeros((6, ROWS), f32)], axis=0).astype(bf16)
    for s in range(GROUP):
        sent_ref[TALL * s : TALL * s + FEAT] = normed
        sent_ref[TALL * s + FEAT : TALL * (s + 1)] = squares


def gate_up(received_ref, wg_ref, wu_ref, own_ref, sent_ref):
    rows = jnp.concatenate(
        [received_ref[TALL * s : TALL * s + FEAT] for s in range(GROUP)], axis=0
    )
    squares = sum(
        received_ref[TALL * s + FEAT : TALL * (s + 1)].astype(f32) for s in range(GROUP)
    )
    total = squares[0:1] + squares[1:2]
    high, low = high_low(total)
    for at, ref in ((0, wg_ref), (HIDDEN, wu_ref)):
        part = dot(ref[...], rows)
        own_ref[at : at + HIDDEN] = part
        sent_ref[at : at + HIDDEN] = part.astype(bf16)
    own_ref[BOTH:] = jnp.broadcast_to(total, (8, ROWS))
    sent_ref[BOTH:] = jnp.concatenate([high, low, jnp.zeros((6, ROWS), f32)], axis=0).astype(bf16)


def down(own_ref, other_ref, w_ref, after_ref, out_ref):
    del after_ref
    squares = other_ref[BOTH:].astype(f32)
    total = own_ref[BOTH : BOTH + 1] + squares[0:1] + squares[1:2]
    scale = lax.rsqrt(total / D + norm_epsilon)
    gate = (own_ref[:HIDDEN] + other_ref[:HIDDEN].astype(f32)) * scale
    up = (own_ref[HIDDEN:BOTH] + other_ref[HIDDEN:BOTH].astype(f32)) * scale
    active = (silu(gate) * up).astype(bf16)
    out_ref[...] = dot(w_ref[...], active, TN).astype(bf16)


def finish(received_ref, middle_ref, out_ref):
    parts = [received_ref[FEAT * s : FEAT * (s + 1)].astype(f32) for s in range(GROUP)]
    while len(parts) > 1:
        parts = [a + b for a, b in zip(parts[::2], parts[1::2])]
    out_ref[...] = (middle_ref[...].astype(f32) + parts[0]).astype(bf16)


def from_other_core(array):
    return lax.ppermute(array, "tp", [(0, 1), (1, 0)])


def over_group(array):
    tiles = array.reshape(GROUP, array.shape[0] // GROUP, array.shape[1])
    return lax.all_to_all(tiles, KV, 0, 0, tiled=True).reshape(array.shape)


def local(
    tokens,
    delta_state,
    gain_in,
    w_query,
    w_key,
    w_value,
    w_out_gate,
    w_beta,
    w_decay,
    decay_rate,
    head_gain,
    w_mix,
    gain_mid,
    w_gate,
    w_up,
    w_down,
):
    v, a = in_vmem(), anywhere()
    own_tokens = tokens.T
    other_tokens = from_other_core(own_tokens)
    summand = kernel(project, "project", shape((ROWS, PIECE), bf16), [v] * 9)(
        own_tokens,
        other_tokens,
        gain_in.reshape(1, 128),
        w_query,
        w_key,
        w_value,
        w_out_gate,
        w_beta.T,
        w_decay.T,
    )
    pieces = over_group(summand)
    mixed, key, correction, keep = kernel(
        mixer,
        "mixer",
        [
            shape((ROWS, WIDTH_DEV), bf16),
            shape((OWN, WIDTH_DEV), f32),
            shape((OWN, WIDTH_DEV), f32),
            shape((OWN, HEAD_DIM), f32),
        ],
        [v] * 4,
    )(pieces, delta_state, decay_rate.reshape(1, HEADS_DEV), head_gain.reshape(1, HEAD_DIM))
    mixed_rows = over_group(mixed)
    own_part, sent_part = kernel(
        mix, "mix", [shape((FEAT, ROWS), f32), shape((FEAT, ROWS), bf16)], [v] * 2
    )(mixed_rows, w_mix)
    middle, sent = kernel(
        middle_rows,
        "middle_rows",
        [shape((FEAT, ROWS), bf16), shape((GROUP * TALL, ROWS), bf16)],
        [v] * 4,
    )(own_tokens, own_part, from_other_core(sent_part), gain_mid.reshape(1, 128))
    received = over_group(sent)
    own_sum, sent_sum = kernel(
        gate_up,
        "gate_up",
        [shape((BOTH + 8, ROWS), f32), shape((BOTH + 8, ROWS), bf16)],
        [v] * 3,
    )(received, w_gate.T, w_up.T)
    block = pl.BlockSpec((1, HEADS_DEV, HEAD_DIM, HEAD_DIM), lambda b: (b, 0, 0, 0))
    next_state = pl.pallas_call(
        update,
        grid=(OWN,),
        out_shape=shape(delta_state.shape, f32),
        in_specs=[block, v, v, v, a],
        out_specs=block,
        name="update",
        compiler_params=pltpu.CompilerParams(vmem_limit_bytes=8 * 1024 * 1024),
    )(delta_state, key, correction, keep, received)
    down_local = kernel(down, "down", shape((GROUP * FEAT, ROWS), bf16), [v, v, v, a])(
        own_sum, from_other_core(sent_sum), w_down, next_state
    )
    layer_out = kernel(finish, "finish", shape((FEAT, ROWS), bf16), [v] * 2)(
        over_group(down_local), middle
    )
    return (layer_out.T, next_state)


def solution(mesh):
    split = Mesh(
        mesh.devices.reshape(mesh.shape["dp"], 4, 4, mesh.shape["tp"]), ("dp", "kv_0", "kv_1", "tp")
    )
    in_specs = (
        P("dp", KV_TP),
        P(DP_KV, "tp", None, None),
        P(KV),
        P(KV, "tp"),
        P(KV, "tp"),
        P(KV, "tp"),
        P(KV, "tp"),
        P(KV, None),
        P(KV, None),
        P("tp"),
        P(),
        P("tp", KV),
        P(KV),
        P("tp", KV),
        P("tp", KV),
        P(KV, "tp"),
    )
    out_specs = (P("dp", KV_TP), P(DP_KV, "tp", None, None))
    return jax.shard_map(local, mesh=split, in_specs=in_specs, out_specs=out_specs, check_vma=False)
```

time: 82.9 us -> 75.2 us (0.907)
  blocking collectives: 0 us -> 51.4 us
  waiting for transfers between devices: 35.9 us -> 1.89 us
  starting transfers between devices: 24.2 us -> 5.92 us
  matrix products: 10.9 us -> 0 us
  Pallas kernels: 0 us -> 6.73 us
  other arithmetic: 5.95 us -> 0 us
  local copies, waits for them, and re-layouts: 4.22 us -> 7.98 us
    all_to_all x0 -> x4, blocking collectives: none -> 51.4 us  [over_group(): return lax.all_to_all(tiles, KV, 0, 0, tiled=True).reshape(array.shape)]
    all_to_all x4 -> x0, waiting for transfers between devices: 33.4 us -> none  [the longest x2 15.5 us: from_everyone(): return lax.all_to_all(copies, axis, split_axis=0, concat_axis=0, tiled=True)]
    all_to_all x4 -> x0, starting transfers between devices: 18.5 us -> none  [the longest x1 7.88 us: local(): pieces = lax.all_to_all(summand, KV, 0, 0, tiled=True)]
    dot_general x12 -> x0, matrix products: 10.9 us -> none  [the longest x6 6.63 us: local(): jnp.dot(normed, weight, preferred_element_type=jnp.float32)]
    unnamed x14 -> x36, local copies, waits for them, and re-layouts: 0.04 us -> 7.98 us
    pallas_call x0 -> x8, Pallas kernels: none -> 6.73 us  [the longest x1 3.7 us: local(): pl.pallas_call(update, grid=(OWN,), out_shape=shape(delta_state.shape, f3...]
    add x1 -> x0, other arithmetic: 1.72 us -> none  [mixer_core(): keep_rate[..., None, None] * delta_state]
    convert_element_type x9 -> x0, other arithmetic: 1.54 us -> none  [the longest x1 0.66 us: local(): normed = (whole_rows * gain_in.astype(jnp.float32)).astype(jnp.bfloat16)]
  transfers between devices with their start and end apart: 8 -> 3, of which waited for: 7 -> 2; matrix products, arithmetic and copies ran while one was open for 7% -> 0% of each run, Pallas kernels for 0% -> 5%
where the time goes in v2:
time: 75.2 us; the launch traced here: 74.7 us
  blocking collectives  51.4 us (68%)
  local copies, waits for them, and re-layouts  7.98 us (11%)
  Pallas kernels  6.73 us (9%)
  starting transfers between devices  5.92 us (8%)
  waiting for transfers between devices  1.89 us (3%)
    all_to_all x4, blocking collectives, over_group(): return lax.all_to_all(tiles, KV, 0, 0, tiled=True).reshape(array.shape)  51.4 us
    unnamed x36, local copies, waits for them, and re-layouts  7.98 us
    ppermute x3, starting transfers between devices, from_other_core(): return lax.ppermute(array, 'tp', [(0, 1), (1, 0)])  5.92 us
    pallas_call x1, Pallas kernels, local(): pl.pallas_call(update, grid=(OWN,), out_shape=shape(delta_state.shape, f3...  3.7 us
    ppermute x3, waiting for transfers between devices, from_other_core(): return lax.ppermute(array, 'tp', [(0, 1), (1, 0)])  1.89 us
  transfers between devices with their start and end apart: 3, of which 2 were waited for; matrix products, arithmetic and copies ran while one was open for 0% of the time, Pallas kernels for 5%

profile of v2, /device:TPU:1, one launch (start us, length us, event | category | flops | bytes accessed | tf_op | source)
XLA Modules:
  0.0 74.7 jit_solution(1426190927179789855)
XLA Ops:
  0.6 1.5 %collective-permute-start = (bf16[64,128]{1,0:T(8,128)(2,1)}, bf16[64,128]{1,0:T(8,128)(2,1)S(1)}, u32[]{:S(2)}, u32[]{:S(2)}) collective-permute-start(bf16[64,128]{1,0:T(8,128)(2,1)} %bitcast.29), channel_id=1, source_target_pairs={{0,1},{1,0},{2,3},{3,2},{4,5},{5,4},{6,7},{7,6},{8,9},{9,8},{10,11... | collective-permute-start | bytes 49160 | tf_op jit(solution)/shard_map/ppermute | solution.py:226
  2.1 1.0 %collective-permute-done.other_ref = bf16[64,128]{1,0:T(8,128)(2,1)S(1)} collective-permute-done((bf16[64,128]{1,0:T(8,128)(2,1)}, bf16[64,128]{1,0:T(8,128)(2,1)S(1)}, u32[]{:S(2)}, u32[]{:S(2)}) %collective-permute-start) | collective-permute-done | bytes 16416 | tf_op jit(solution)/shard_map/ppermute | solution.py:226
  3.2 0.9 %copy-done.6 = bf16[128,512]{1,0:T(8,128)(2,1)S(1)} copy-done((bf16[128,512]{1,0:T(8,128)(2,1)S(1)}, bf16[128,512]{1,0:T(8,128)(2,1)}, u32[]{:S(2)}) %copy-start.6) | copy-done | bytes 131096
  4.1 0.9 %copy-done.7 = bf16[128,512]{1,0:T(8,128)(2,1)S(1)} copy-done((bf16[128,512]{1,0:T(8,128)(2,1)S(1)}, bf16[128,512]{1,0:T(8,128)(2,1)}, u32[]{:S(2)}) %copy-start.7) | copy-done | bytes 131096
  5.0 0.9 %copy-done.8 = bf16[128,512]{1,0:T(8,128)(2,1)S(1)} copy-done((bf16[128,512]{1,0:T(8,128)(2,1)S(1)}, bf16[128,512]{1,0:T(8,128)(2,1)}, u32[]{:S(2)}) %copy-start.8) | copy-done | bytes 131096
  5.9 0.9 %copy-done.9 = bf16[128,512]{1,0:T(8,128)(2,1)S(1)} copy-done((bf16[128,512]{1,0:T(8,128)(2,1)S(1)}, bf16[128,512]{1,0:T(8,128)(2,1)}, u32[]{:S(2)}) %copy-start.9) | copy-done | bytes 131096
  6.8 0.7 copy-done.10
  7.5 0.7 copy-done.12
  8.2 0.7 copy-done.13
  8.9 0.7 copy-done.14
  9.5 0.4 project.1
  9.9 19.0 %all_to_all.20 = bf16[16,8,2176]{2,1,0:T(8,128)(2,1)S(1)} all-to-all(bf16[16,8,2176]{2,1,0:T(8,128)(2,1)S(1)} %bitcast.21), channel_id=1, replica_groups=mesh['dp'=4,'kv_0'=4,'kv_1'=4,'tp'=2] {'kv_0','kv_1'}, dimensions={0} | all-to-all | bytes 1114112 | tf_op jit(solution)/shard_map/all_to_all | solution.py:231
  28.9 0.7 mixer.1
  29.6 10.1 %all_to_all.21 = bf16[16,8,512]{2,1,0:T(8,128)(2,1)S(1)} all-to-all(bf16[16,8,512]{2,1,0:T(8,128)(2,1)S(1)} %bitcast.28), channel_id=1, replica_groups=mesh['dp'=4,'kv_0'=4,'kv_1'=4,'tp'=2] {'kv_0','kv_1'}, dimensions={0} | all-to-all | bytes 262144 | tf_op jit(solution)/shard_map/all_to_all | solution.py:231
  39.9 2.9 %collective-permute-start.1 = (bf16[64,128]{1,0:T(8,128)(2,1)S(1)}, bf16[64,128]{1,0:T(8,128)(2,1)S(1)}, u32[]{:S(2)}, u32[]{:S(2)}) collective-permute-start(bf16[64,128]{1,0:T(8,128)(2,1)S(1)} %get-tuple-element.14), channel_id=1, source_target_pairs={{0,1},{1,0},{2,3},{3,2},{4,5},{5,4},{6,7},{7,6},{8,9},{9,8},{10,11... | collective-permute-start | bytes 49160 | tf_op jit(solution)/shard_map/ppermute | solution.py:226
  42.8 0.8 %collective-permute-done.1.other_ref = bf16[64,128]{1,0:T(8,128)(2,1)S(1)} collective-permute-done((bf16[64,128]{1,0:T(8,128)(2,1)S(1)}, bf16[64,128]{1,0:T(8,128)(2,1)S(1)}, u32[]{:S(2)}, u32[]{:S(2)}) %collective-permute-start.1) | collective-permute-done | bytes 16416 | tf_op jit(solution)/shard_map/ppermute | solution.py:226
  43.8 11.3 %all_to_all.22 = bf16[16,72,128]{2,1,0:T(8,128)(2,1)S(1)} all-to-all(bf16[16,72,128]{2,1,0:T(8,128)(2,1)S(1)} %bitcast.27), channel_id=1, replica_groups=mesh['dp'=4,'kv_0'=4,'kv_1'=4,'tp'=2] {'kv_0','kv_1'}, dimensions={0} | all-to-all | bytes 589824 | tf_op jit(solution)/shard_map/all_to_all | solution.py:231
  55.1 0.5 gate_up.1
  55.6 1.6 %collective-permute-start.2 = (bf16[712,128]{1,0:T(8,128)(2,1)S(1)}, bf16[712,128]{1,0:T(8,128)(2,1)S(1)}, u32[]{:S(2)}, u32[]{:S(2)}) collective-permute-start(bf16[712,128]{1,0:T(8,128)(2,1)S(1)} %get-tuple-element.17), channel_id=1, source_target_pairs={{0,1},{1,0},{2,3},{3,2},{4,5},{5,4},{6,7},{7,6},{8,9},{9,8},{10,11... | collective-permute-start | bytes 546824 | tf_op jit(solution)/shard_map/ppermute | solution.py:226
  57.2 3.7 %update.1.after_ref = f32[8,4,128,128]{3,2,1,0:T(8,128)} custom-call(f32[8,4,128,128]{3,2,1,0:T(8,128)S(1)} %copy-done, f32[8,512]{1,0:T(8,128)S(1)} %get-tuple-element.18.key_ref, f32[8,512]{1,0:T(8,128)S(1)} %get-tuple-element.19.correct_ref, f32[8,128]{1,0:T(8,128)S(1)} %get-tuple-element.20.keep_ref, bf16[1152,128]{1,0:T(8,128)(2,1)S(1)} %bitcast.19), custom_call_target="tpu_custom_call" | custom-call | tf_op jit(solution)/shard_map/update/pallas_call | solution.py:296
  60.9 1.6 %copy-done.1 = f32[8,4,128,128]{3,2,1,0:T(8,128)S(1)} copy-done((f32[8,4,128,128]{3,2,1,0:T(8,128)S(1)}, f32[8,4,128,128]{3,2,1,0:T(8,128)}, u32[]{:S(2)}) %copy-start.1) | copy-done | bytes 2097176
  62.5 0.4 down.1
  63.0 11.1 %all_to_all.23 = bf16[16,64,128]{2,1,0:T(8,128)(2,1)S(1)} all-to-all(bf16[16,64,128]{2,1,0:T(8,128)(2,1)S(1)} %bitcast.23), channel_id=1, replica_groups=mesh['dp'=4,'kv_0'=4,'kv_1'=4,'tp'=2] {'kv_0','kv_1'}, dimensions={0} | all-to-all | bytes 524288 | tf_op jit(solution)/shard_map/all_to_all | solution.py:231
  74.0 0.6 finish.1
  (30 shorter events, 0.4 us)
Async XLA Ops:
  0.6 28.3 %copy-start = (f32[8,4,128,128]{3,2,1,0:T(8,128)S(1)}, f32[8,4,128,128]{3,2,1,0:T(8,128)}, u32[]{:S(2)}) copy-start(f32[8,4,128,128]{3,2,1,0:T(8,128)} %state_ref.3) | copy-start | bytes 6291460
  0.6 2.5 %collective-permute-start = (bf16[64,128]{1,0:T(8,128)(2,1)}, bf16[64,128]{1,0:T(8,128)(2,1)S(1)}, u32[]{:S(2)}, u32[]{:S(2)}) collective-permute-start(bf16[64,128]{1,0:T(8,128)(2,1)} %bitcast.29), channel_id=1, source_target_pairs={{0,1},{1,0},{2,3},{3,2},{4,5},{5,4},{6,7},{7,6},{8,9},{9,8},{10,11... | collective-permute-start | bytes 49160 | tf_op jit(solution)/shard_map/ppermute | solution.py:226
  3.2 0.9 %copy-start.6 = (bf16[128,512]{1,0:T(8,128)(2,1)S(1)}, bf16[128,512]{1,0:T(8,128)(2,1)}, u32[]{:S(2)}) copy-start(bf16[128,512]{1,0:T(8,128)(2,1)} %wq_ref.1) | copy-start | bytes 393220
  4.1 0.9 %copy-start.7 = (bf16[128,512]{1,0:T(8,128)(2,1)S(1)}, bf16[128,512]{1,0:T(8,128)(2,1)}, u32[]{:S(2)}) copy-start(bf16[128,512]{1,0:T(8,128)(2,1)} %wk_ref.1) | copy-start | bytes 393220
  5.0 0.9 %copy-start.8 = (bf16[128,512]{1,0:T(8,128)(2,1)S(1)}, bf16[128,512]{1,0:T(8,128)(2,1)}, u32[]{:S(2)}) copy-start(bf16[128,512]{1,0:T(8,128)(2,1)} %wv_ref.1) | copy-start | bytes 393220
  5.9 0.9 %copy-start.9 = (bf16[128,512]{1,0:T(8,128)(2,1)S(1)}, bf16[128,512]{1,0:T(8,128)(2,1)}, u32[]{:S(2)}) copy-start(bf16[128,512]{1,0:T(8,128)(2,1)} %wg_ref.1) | copy-start | bytes 393220
  6.8 0.7 copy-start.10
  7.5 0.7 copy-start.12
  8.2 0.7 copy-start.13
  8.9 0.7 copy-start.14
  9.5 19.4 %copy-start.15 = (f32[4]{0:T(128)S(1)}, f32[4]{0:T(128)}, u32[]{:S(2)}) copy-start(f32[4]{0:T(128)} %param.25) | copy-start | bytes 52
  9.5 19.4 %copy-start.16 = (f32[128]{0:T(128)S(1)}, f32[128]{0:T(128)}, u32[]{:S(2)}) copy-start(f32[128]{0:T(128)} %param.26) | copy-start | bytes 1540
  9.9 29.8 %copy-start.5 = (bf16[512,128]{1,0:T(8,128)(2,1)S(1)}, bf16[512,128]{1,0:T(8,128)(2,1)}, u32[]{:S(2)}) copy-start(bf16[512,128]{1,0:T(8,128)(2,1)} %w_ref.2) | copy-start | bytes 393220
  9.9 33.8 %copy-start.11 = (bf16[128,64]{0,1:T(8,128)(2,1)S(1)}, bf16[128,64]{0,1:T(8,128)(2,1)}, u32[]{:S(2)}) copy-start(bf16[128,64]{0,1:T(8,128)(2,1)} %param.16) | copy-start | bytes 49156
  9.9 33.8 %copy-start.17 = (bf16[128]{0:T(256)(128)(2,1)S(1)}, bf16[128]{0:T(256)(128)(2,1)}, u32[]{:S(2)}) copy-start(bf16[128]{0:T(256)(128)(2,1)} %param.28) | copy-start | bytes 772
  28.9 26.2 %copy-start.2 = (bf16[1024,352]{0,1:T(8,128)(2,1)S(1)}, bf16[1024,352]{0,1:T(8,128)(2,1)}, u32[]{:S(2)}) copy-start(bf16[1024,352]{0,1:T(8,128)(2,1)} %param.29) | copy-start | bytes 2162692
  28.9 26.2 %copy-start.3 = (bf16[1024,352]{0,1:T(8,128)(2,1)S(1)}, bf16[1024,352]{0,1:T(8,128)(2,1)}, u32[]{:S(2)}) copy-start(bf16[1024,352]{0,1:T(8,128)(2,1)} %param.30) | copy-start | bytes 2162692
  39.9 3.7 %collective-permute-start.1 = (bf16[64,128]{1,0:T(8,128)(2,1)S(1)}, bf16[64,128]{1,0:T(8,128)(2,1)S(1)}, u32[]{:S(2)}, u32[]{:S(2)}) collective-permute-start(bf16[64,128]{1,0:T(8,128)(2,1)S(1)} %get-tuple-element.14), channel_id=1, source_target_pairs={{0,1},{1,0},{2,3},{3,2},{4,5},{5,4},{6,7},{7,6},{8,9},{9,8},{10,11... | collective-permute-start | bytes 49160 | tf_op jit(solution)/shard_map/ppermute | solution.py:226
  55.6 5.3 %collective-permute-start.2 = (bf16[712,128]{1,0:T(8,128)(2,1)S(1)}, bf16[712,128]{1,0:T(8,128)(2,1)S(1)}, u32[]{:S(2)}, u32[]{:S(2)}) collective-permute-start(bf16[712,128]{1,0:T(8,128)(2,1)S(1)} %get-tuple-element.17), channel_id=1, source_target_pairs={{0,1},{1,0},{2,3},{3,2},{4,5},{5,4},{6,7},{7,6},{8,9},{9,8},{10,11... | collective-permute-start | bytes 546824 | tf_op jit(solution)/shard_map/ppermute | solution.py:226
  57.2 3.7 %copy-start.4 = (bf16[352,1024]{1,0:T(8,128)(2,1)S(1)}, bf16[352,1024]{1,0:T(8,128)(2,1)}, u32[]{:S(2)}) copy-start(bf16[352,1024]{1,0:T(8,128)(2,1)} %w_ref.3) | copy-start | bytes 2162692
  60.9 1.6 %copy-start.1 = (f32[8,4,128,128]{3,2,1,0:T(8,128)S(1)}, f32[8,4,128,128]{3,2,1,0:T(8,128)}, u32[]{:S(2)}) copy-start(f32[8,4,128,128]{3,2,1,0:T(8,128)} %update.1.after_ref) | copy-start | bytes 6291460

commit v3 on v2

--- a/solution.py
+++ b/solution.py
@@ -1,3 +1,5 @@
+import functools
+
 import jax
 import jax.numpy as jnp
 from jax import lax
@@ -150,19 +152,70 @@
     keep_ref[...] = keeps
 
 
-def update(state_ref, key_ref, correct_ref, keep_ref, after_ref, next_ref):
+HALF = OWN // 2
+
+
+def update(first, state_ref, key_ref, correct_ref, keep_ref, after_ref, *rest):
     del after_ref
-    b = pl.program_id(0)
-    pick = lax.broadcasted_iota(jnp.int32, (OWN, WIDTH_DEV), 0) == b
-    key = jnp.sum(jnp.where(pick, key_ref[...], 0.0), axis=0, keepdims=True)
-    correction = jnp.sum(jnp.where(pick, correct_ref[...], 0.0), axis=0, keepdims=True)
-    keep = jnp.sum(jnp.where(pick[:, :HEAD_DIM], keep_ref[...], 0.0), axis=0, keepdims=True)
-    for h in range(HEADS_DEV):
-        at = h * HEAD_DIM
-        key_column = jnp.broadcast_to(key[:, at : at + HEAD_DIM], (HEAD_DIM, HEAD_DIM)).T
-        next_ref[0, h] = (
-            keep[:, h : h + 1] * state_ref[0, h] + key_column * correction[:, at : at + HEAD_DIM]
-        )
+    next_ref, token_ref, made_ref, sems = rest[-4:]
+    copies = []
+    for b in range(HALF):
+        row = first + b
+        for h in range(HEADS_DEV):
+            at = h * HEAD_DIM
+            key = key_ref[row : row + 1, at : at + HEAD_DIM]
+            key_column = jnp.broadcast_to(key, (HEAD_DIM, HEAD_DIM)).T
+            made_ref[b, h] = (
+                keep_ref[row : row + 1, h : h + 1] * state_ref[row, h]
+                + key_column * correct_ref[row : row + 1, at : at + HEAD_DIM]
+            )
+        copies.append(pltpu.make_async_copy(made_ref.at[b], next_ref.at[row], sems.at[b]))
+        copies[-1].start()
+    token_ref[...] = jnp.zeros(token_ref.shape, f32)
+    for copy in copies:
+        copy.wait()
+
+
+def updated(first, state, key, correction, keep, after, base=None):
+    operands = [state, key, correction, keep, after] + ([] if base is None else [base])
+    hbm = pl.BlockSpec(memory_space=pltpu.HBM)
+    return pl.pallas_call(
+        functools.partial(update, first),
+        out_shape=[shape(state.shape, f32), shape((8, 128), f32)],
+        in_specs=[in_vmem()] * 4 + [anywhere()] + ([] if base is None else [hbm]),
+        out_specs=[hbm, in_vmem()],
+        scratch_shapes=[
+            pltpu.VMEM((HALF, HEADS_DEV, HEAD_DIM, HEAD_DIM), f32),
+            pltpu.SemaphoreType.DMA((HALF,)),
+        ],
+        input_output_aliases={} if base is None else {5: 0},
+        name="update",
+        compiler_params=pltpu.CompilerParams(vmem_limit_bytes=12 * 1024 * 1024),
+    )(*operands)
+
+
+def preload(*refs):
+    count = (len(refs) - 1) // 2
+    sems = refs[-1]
+    copies = [
+        pltpu.make_async_copy(refs[i], refs[count + i], sems.at[i]) for i in range(count)
+    ]
+    for copy in copies:
+        copy.start()
+    for copy in copies:
+        copy.wait()
+
+
+def preloaded(*arrays):
+    return pl.pallas_call(
+        preload,
+        out_shape=[shape(x.shape, x.dtype) for x in arrays],
+        in_specs=[pl.BlockSpec(memory_space=pltpu.HBM)] * len(arrays),
+        out_specs=[in_vmem() for _ in arrays],
+        scratch_shapes=[pltpu.SemaphoreType.DMA((len(arrays),))],
+        name="preload",
+        compiler_params=pltpu.CompilerParams(vmem_limit_bytes=4 * 1024 * 1024),
+    )(*(pltpu.with_memory_space_constraint(x, pltpu.HBM) for x in arrays))
 
 
 def mix(mixed_ref, w_ref, own_ref, sent_ref):
@@ -172,7 +225,8 @@
     sent_ref[...] = jnp.where(on_first, part[FEAT:], part[:FEAT]).astype(bf16)
 
 
-def middle_rows(tokens_ref, own_ref, other_ref, gain_ref, middle_ref, sent_ref):
+def middle_rows(tokens_ref, own_ref, other_ref, gain_ref, after_ref, middle_ref, sent_ref):
+    del after_ref
     on_first = lax.axis_index("tp") == 0
     gains = jnp.broadcast_to(gain_ref[...].astype(f32), (128, 128)).T
     gain = jnp.where(on_first, gains[:FEAT], gains[FEAT:])
@@ -252,9 +306,8 @@
     v, a = in_vmem(), anywhere()
     own_tokens = tokens.T
     other_tokens = from_other_core(own_tokens)
-    summand = kernel(project, "project", shape((ROWS, PIECE), bf16), [v] * 9)(
+    loaded = preloaded(
         own_tokens,
-        other_tokens,
         gain_in.reshape(1, 128),
         w_query,
         w_key,
@@ -262,6 +315,9 @@
         w_out_gate,
         w_beta.T,
         w_decay.T,
+    )
+    summand = kernel(project, "project", shape((ROWS, PIECE), bf16), [v] * 9)(
+        loaded[0], other_tokens, *loaded[1:]
     )
     pieces = over_group(summand)
     mixed, key, correction, keep = kernel(
@@ -279,12 +335,13 @@
     own_part, sent_part = kernel(
         mix, "mix", [shape((FEAT, ROWS), f32), shape((FEAT, ROWS), bf16)], [v] * 2
     )(mixed_rows, w_mix)
+    half_state, half_token = updated(0, delta_state, key, correction, keep, mixed_rows)
     middle, sent = kernel(
         middle_rows,
         "middle_rows",
         [shape((FEAT, ROWS), bf16), shape((GROUP * TALL, ROWS), bf16)],
-        [v] * 4,
-    )(own_tokens, own_part, from_other_core(sent_part), gain_mid.reshape(1, 128))
+        [v] * 4 + [a],
+    )(loaded[0], own_part, from_other_core(sent_part), gain_mid.reshape(1, 128), half_token)
     received = over_group(sent)
     own_sum, sent_sum = kernel(
         gate_up,
@@ -292,18 +349,9 @@
         [shape((BOTH + 8, ROWS), f32), shape((BOTH + 8, ROWS), bf16)],
         [v] * 3,
     )(received, w_gate.T, w_up.T)
-    block = pl.BlockSpec((1, HEADS_DEV, HEAD_DIM, HEAD_DIM), lambda b: (b, 0, 0, 0))
-    next_state = pl.pallas_call(
-        update,
-        grid=(OWN,),
-        out_shape=shape(delta_state.shape, f32),
-        in_specs=[block, v, v, v, a],
-        out_specs=block,
-        name="update",
-        compiler_params=pltpu.CompilerParams(vmem_limit_bytes=8 * 1024 * 1024),
-    )(delta_state, key, correction, keep, received)
+    next_state, token = updated(HALF, delta_state, key, correction, keep, received, half_state)
     down_local = kernel(down, "down", shape((GROUP * FEAT, ROWS), bf16), [v, v, v, a])(
-        own_sum, from_other_core(sent_sum), w_down, next_state
+        own_sum, from_other_core(sent_sum), w_down, token
     )
     layer_out = kernel(finish, "finish", shape((FEAT, ROWS), bf16), [v] * 2)(
         over_group(down_local), middle

time: 75.2 us -> 65 us (0.86)
  local copies, waits for them, and re-layouts: 7.98 us -> 0.05 us
  waiting for transfers between devices: 1.89 us -> 0.01 us
    unnamed x36 -> x16, local copies, waits for them, and re-layouts: 7.98 us -> 0.05 us
    ppermute x3, waiting for transfers between devices: 1.89 us -> 0.01 us  [from_other_core(): return lax.ppermute(array, 'tp', [(0, 1), (1, 0)])]
    pallas_call x1 -> x3, Pallas kernels: 3.7 us -> 3.55 us  [the longest x2 2.36 us: updated(): pl.pallas_call(functools.partial(update, first), out_shape=[shape(state.s...]
  transfers between devices with their start and end apart: 3 -> 3, of which waited for: 2 -> 0; matrix products, arithmetic and copies ran while one was open for 0% -> 0% of each run, Pallas kernels for 5% -> 5%
where the time goes in v3:
time: 65 us; the launch traced here: 64.8 us
  blocking collectives  51.7 us (80%)
  Pallas kernels  6.61 us (10%)
  starting transfers between devices  5.55 us (9%)
  between operations  0.8 us (1%)
    all_to_all x4, blocking collectives, over_group(): return lax.all_to_all(tiles, KV, 0, 0, tiled=True).reshape(array.shape)  51.7 us
    ppermute x3, starting transfers between devices, from_other_core(): return lax.ppermute(array, 'tp', [(0, 1), (1, 0)])  5.55 us
    pallas_call x2, Pallas kernels, updated(): pl.pallas_call(functools.partial(update, first), out_shape=[shape(state.s...  2.36 us
  transfers between devices with their start and end apart: 3, of which 0 were waited for; matrix products, arithmetic and copies ran while one was open for 0% of the time, Pallas kernels for 5%

profile of v3, /device:TPU:1, one launch (start us, length us, event | category | flops | bytes accessed | tf_op | source)
XLA Modules:
  0.0 64.8 jit_solution(7094399109597886107)
XLA Ops:
  0.7 1.5 %collective-permute-start = (bf16[64,128]{1,0:T(8,128)(2,1)}, bf16[64,128]{1,0:T(8,128)(2,1)S(1)}, u32[]{:S(2)}, u32[]{:S(2)}) collective-permute-start(bf16[64,128]{1,0:T(8,128)(2,1)} %bitcast.33), channel_id=1, source_target_pairs={{0,1},{1,0},{2,3},{3,2},{4,5},{5,4},{6,7},{7,6},{8,9},{9,8},{10,11... | collective-permute-start | bytes 49160 | tf_op jit(solution)/shard_map/ppermute | solution.py:280
  2.1 1.2 %preload.1 = (bf16[64,128]{1,0:T(8,128)(2,1)S(1)}, bf16[1,128]{1,0:T(2,128)(2,1)S(1)}, bf16[128,512]{1,0:T(8,128)(2,1)S(1)}, bf16[128,512]{1,0:T(8,128)(2,1)S(1)...) custom-call(bf16[64,128]{1,0:T(8,128)(2,1)} %bitcast.34, ...), custom_call_target="tpu_custom_call" | custom-call | tf_op jit(solution)/shard_map/preload/pallas_call | solution.py:210
  3.3 0.0 collective-permute-done.other_ref
  3.3 0.4 project.1
  3.7 0.0 copy-start.4
  3.7 19.1 %all_to_all.20 = bf16[16,8,2176]{2,1,0:T(8,128)(2,1)S(1)} all-to-all(bf16[16,8,2176]{2,1,0:T(8,128)(2,1)S(1)} %bitcast.21), channel_id=1, replica_groups=mesh['dp'=4,'kv_0'=4,'kv_1'=4,'tp'=2] {'kv_0','kv_1'}, dimensions={0} | all-to-all | bytes 1114112 | tf_op jit(solution)/shard_map/all_to_all | solution.py:285
  22.8 0.0 copy-start.7
  22.8 0.7 %mixer.1 = (bf16[128,512]{1,0:T(8,128)(2,1)S(1)}, f32[8,512]{1,0:T(8,128)S(1)}, f32[8,512]{1,0:T(8,128)S(1)}, f32[8,128]{1,0:T(8,128)S(1)}) custom-call(bf16[128,2176]{1,0:T(8,128)(2,1)S(1)} %bitcast.20, f32[8,4,128,128]{3,2,1,0:T(8,128)S(1)} %copy-done, f32[1,4]{1,0:T(1,128)S(1)} %bitcast.30, f32[1,128]{1,0:T(1,128)S(1)} %bitcast.31), custom_call_target="tpu_custom_call" | custom-call | tf_op jit(solution)/shard_map/mixer/pallas_call | solution.py:323
  23.5 0.0 copy-start.1
  23.5 0.0 copy-start.2
  23.5 10.1 %all_to_all.21 = bf16[16,8,512]{2,1,0:T(8,128)(2,1)S(1)} all-to-all(bf16[16,8,512]{2,1,0:T(8,128)(2,1)S(1)} %bitcast.29), channel_id=1, replica_groups=mesh['dp'=4,'kv_0'=4,'kv_1'=4,'tp'=2] {'kv_0','kv_1'}, dimensions={0} | all-to-all | bytes 262144 | tf_op jit(solution)/shard_map/all_to_all | solution.py:285
  33.7 0.2 mix.1
  33.9 2.9 %collective-permute-start.1 = (bf16[64,128]{1,0:T(8,128)(2,1)S(1)}, bf16[64,128]{1,0:T(8,128)(2,1)S(1)}, u32[]{:S(2)}, u32[]{:S(2)}) collective-permute-start(bf16[64,128]{1,0:T(8,128)(2,1)S(1)} %get-tuple-element.34), channel_id=1, source_target_pairs={{0,1},{1,0},{2,3},{3,2},{4,5},{5,4},{6,7},{7,6},{8,9},{9,8},{10,11... | collective-permute-start | bytes 49160 | tf_op jit(solution)/shard_map/ppermute | solution.py:280
  36.8 1.2 %update.2 = (f32[8,4,128,128]{3,2,1,0:T(8,128)}, f32[8,128]{1,0:T(8,128)S(1)}) custom-call(f32[8,4,128,128]{3,2,1,0:T(8,128)S(1)} %copy-done, f32[8,512]{1,0:T(8,128)S(1)} %get-tuple-element.35.key_ref, f32[8,512]{1,0:T(8,128)S(1)} %get-tuple-element.36.correct_ref, f32[8,128]{1,0:T(8,128)S(1)} %get-tuple-element.37.keep_ref, bf16[128,512]{1,0:T(8,128)(2,1)S(1)} %bitcast.23), custom_call_target="tpu_custom_call" | custom-call | tf_op jit(solution)/shard_map/update/pallas_call | solution.py:182
  38.0 0.0 collective-permute-done.1.other_ref
  38.0 0.1 middle_rows.1
  38.1 11.6 %all_to_all.22 = bf16[16,72,128]{2,1,0:T(8,128)(2,1)S(1)} all-to-all(bf16[16,72,128]{2,1,0:T(8,128)(2,1)S(1)} %bitcast.28), channel_id=1, replica_groups=mesh['dp'=4,'kv_0'=4,'kv_1'=4,'tp'=2] {'kv_0','kv_1'}, dimensions={0} | all-to-all | bytes 589824 | tf_op jit(solution)/shard_map/all_to_all | solution.py:285
  49.8 0.5 gate_up.1
  50.3 1.2 %collective-permute-start.2 = (bf16[712,128]{1,0:T(8,128)(2,1)S(1)}, bf16[712,128]{1,0:T(8,128)(2,1)S(1)}, u32[]{:S(2)}, u32[]{:S(2)}) collective-permute-start(bf16[712,128]{1,0:T(8,128)(2,1)S(1)} %get-tuple-element.41), channel_id=1, source_target_pairs={{0,1},{1,0},{2,3},{3,2},{4,5},{5,4},{6,7},{7,6},{8,9},{9,8},{10,11... | collective-permute-start | bytes 546824 | tf_op jit(solution)/shard_map/ppermute | solution.py:280
  51.5 1.2 %update.3 = (f32[8,4,128,128]{3,2,1,0:T(8,128)}, f32[8,128]{1,0:T(8,128)S(1)}) custom-call(f32[8,4,128,128]{3,2,1,0:T(8,128)S(1)} %copy-done, f32[8,512]{1,0:T(8,128)S(1)} %get-tuple-element.35.key_ref, f32[8,512]{1,0:T(8,128)S(1)} %get-tuple-element.36.correct_ref, f32[8,128]{1,0:T(8,128)S(1)} %get-tuple-element.37.keep_ref, ...), custom_call_target="tpu_custom_call", output_to_operand_aliasing={{0}: (5, {})} | custom-call | tf_op jit(solution)/shard_map/update/pallas_call | solution.py:182
  52.7 0.0 collective-permute-done.2.other_ref
  52.7 0.5 down.1
  53.2 10.9 %all_to_all.23 = bf16[16,64,128]{2,1,0:T(8,128)(2,1)S(1)} all-to-all(bf16[16,64,128]{2,1,0:T(8,128)(2,1)S(1)} %bitcast.25), channel_id=1, replica_groups=mesh['dp'=4,'kv_0'=4,'kv_1'=4,'tp'=2] {'kv_0','kv_1'}, dimensions={0} | all-to-all | bytes 524288 | tf_op jit(solution)/shard_map/all_to_all | solution.py:285
  64.1 0.6 %finish.1 = bf16[64,128]{1,0:T(8,128)(2,1)} custom-call(bf16[1024,128]{1,0:T(8,128)(2,1)S(1)} %bitcast.24, bf16[64,128]{1,0:T(8,128)(2,1)S(1)} %get-tuple-element.44.middle_ref), custom_call_target="tpu_custom_call" | custom-call | tf_op jit(solution)/shard_map/finish/pallas_call | solution.py:356
  (12 shorter events, 0.0 us)
Async XLA Ops:
  0.6 22.1 %copy-start = (f32[8,4,128,128]{3,2,1,0:T(8,128)S(1)}, f32[8,4,128,128]{3,2,1,0:T(8,128)}, u32[]{:S(2)}) copy-start(f32[8,4,128,128]{3,2,1,0:T(8,128)} %state_ref.5) | copy-start | bytes 6291460
  0.6 22.1 %copy-start.6 = (f32[128]{0:T(128)S(1)}, f32[128]{0:T(128)}, u32[]{:S(2)}) copy-start(f32[128]{0:T(128)} %param.26) | copy-start | bytes 1540
  0.7 22.1 %copy-start.5 = (f32[4]{0:T(128)S(1)}, f32[4]{0:T(128)}, u32[]{:S(2)}) copy-start(f32[4]{0:T(128)} %param.25) | copy-start | bytes 52
  0.7 2.7 %collective-permute-start = (bf16[64,128]{1,0:T(8,128)(2,1)}, bf16[64,128]{1,0:T(8,128)(2,1)S(1)}, u32[]{:S(2)}, u32[]{:S(2)}) collective-permute-start(bf16[64,128]{1,0:T(8,128)(2,1)} %bitcast.33), channel_id=1, source_target_pairs={{0,1},{1,0},{2,3},{3,2},{4,5},{5,4},{6,7},{7,6},{8,9},{9,8},{10,11... | collective-permute-start | bytes 49160 | tf_op jit(solution)/shard_map/ppermute | solution.py:280
  3.7 30.0 %copy-start.4 = (bf16[512,128]{1,0:T(8,128)(2,1)S(1)}, bf16[512,128]{1,0:T(8,128)(2,1)}, u32[]{:S(2)}) copy-start(bf16[512,128]{1,0:T(8,128)(2,1)} %w_ref.2) | copy-start | bytes 393220
  22.8 15.2 %copy-start.7 = (bf16[128]{0:T(256)(128)(2,1)S(1)}, bf16[128]{0:T(256)(128)(2,1)}, u32[]{:S(2)}) copy-start(bf16[128]{0:T(256)(128)(2,1)} %param.28) | copy-start | bytes 772
  23.5 26.3 %copy-start.1 = (bf16[1024,352]{0,1:T(8,128)(2,1)S(1)}, bf16[1024,352]{0,1:T(8,128)(2,1)}, u32[]{:S(2)}) copy-start(bf16[1024,352]{0,1:T(8,128)(2,1)} %param.29) | copy-start | bytes 2162692
  23.5 26.2 %copy-start.2 = (bf16[1024,352]{0,1:T(8,128)(2,1)S(1)}, bf16[1024,352]{0,1:T(8,128)(2,1)}, u32[]{:S(2)}) copy-start(bf16[1024,352]{0,1:T(8,128)(2,1)} %param.30) | copy-start | bytes 2162692
  33.9 4.0 %collective-permute-start.1 = (bf16[64,128]{1,0:T(8,128)(2,1)S(1)}, bf16[64,128]{1,0:T(8,128)(2,1)S(1)}, u32[]{:S(2)}, u32[]{:S(2)}) collective-permute-start(bf16[64,128]{1,0:T(8,128)(2,1)S(1)} %get-tuple-element.34), channel_id=1, source_target_pairs={{0,1},{1,0},{2,3},{3,2},{4,5},{5,4},{6,7},{7,6},{8,9},{9,8},{10,11... | collective-permute-start | bytes 49160 | tf_op jit(solution)/shard_map/ppermute | solution.py:280
  50.3 2.4 %collective-permute-start.2 = (bf16[712,128]{1,0:T(8,128)(2,1)S(1)}, bf16[712,128]{1,0:T(8,128)(2,1)S(1)}, u32[]{:S(2)}, u32[]{:S(2)}) collective-permute-start(bf16[712,128]{1,0:T(8,128)(2,1)S(1)} %get-tuple-element.41), channel_id=1, source_target_pairs={{0,1},{1,0},{2,3},{3,2},{4,5},{5,4},{6,7},{7,6},{8,9},{9,8},{10,11... | collective-permute-start | bytes 546824 | tf_op jit(solution)/shard_map/ppermute | solution.py:280
  51.5 1.2 %copy-start.3 = (bf16[352,1024]{1,0:T(8,128)(2,1)S(1)}, bf16[352,1024]{1,0:T(8,128)(2,1)}, u32[]{:S(2)}) copy-start(bf16[352,1024]{1,0:T(8,128)(2,1)} %w_ref.3) | copy-start | bytes 2162692

commit v4 on v3

v4 whole, which is shorter than its diff:
```python
import jax
import jax.numpy as jnp
from jax import lax
from jax.experimental import pallas as pl
from jax.experimental.pallas import tpu as pltpu
from jax.sharding import Mesh
from jax.sharding import PartitionSpec as P


D = 2048
HEAD_DIM = 128
KV = ("kv_0", "kv_1")
KV_TP = ("kv_0", "kv_1", "tp")
DP_KV = ("dp", "kv_0", "kv_1")

norm_epsilon = 1e-06
bf16 = jnp.bfloat16
f32 = jnp.float32

GROUP = 16
ROWS = 128
OWN = ROWS // GROUP
FEAT = 64
HEADS_DEV = 4
WIDTH_DEV = HEADS_DEV * HEAD_DIM
SMALL_AT = 4 * WIDTH_DEV
TOKENS_AT = SMALL_AT + 128
PIECE = TOKENS_AT + 128
RING = 4
FEAT_RING = RING * FEAT
SEQ_RING = RING * OWN
MIXED = WIDTH_DEV + FEAT_RING
HIDDEN = 352
BOTH = 2 * HIDDEN

TN = (((0,), (0,)), ((), ()))
NT = (((1,), (1,)), ((), ()))


def in_vmem():
    return pl.BlockSpec(memory_space=pltpu.VMEM)


def anywhere():
    return pl.BlockSpec(memory_space=pl.ANY)


def shape(lengths, dtype):
    return jax.ShapeDtypeStruct(lengths, dtype)


def kernel(body, outs, in_specs, limit=12):
    single = not isinstance(outs, (list, tuple))
    return pl.pallas_call(
        body,
        out_shape=outs,
        in_specs=in_specs,
        out_specs=in_vmem() if single else [in_vmem() for _ in outs],
        compiler_params=pltpu.CompilerParams(vmem_limit_bytes=limit * 1024 * 1024),
    )


def silu(value):
    return value / (1.0 + jnp.exp(-value))


def high_low(value):
    high = value.astype(bf16).astype(f32)
    return high, value - high


def dot(left, right, dims=(((1,), (0,)), ((), ()))):
    return lax.dot_general(left, right, dims, preferred_element_type=f32)


def half_turn(value):
    return pltpu.roll(value, 64, 1)


def project(
    own_ref, gain_ref, gain_mid_ref, wq_ref, wk_ref, wv_ref, wg_ref, wb_ref, wd_ref, other_ref, after_ref, out_ref
):
    del after_ref
    on_first = lax.axis_index("tp") == 0
    own = own_ref[...].astype(f32)
    other = other_ref[...].astype(f32)
    rows = jnp.concatenate(
        [jnp.where(on_first, own, other), jnp.where(on_first, other, own)], axis=0
    ).T
    out_ref[:, TOKENS_AT:] = rows.astype(bf16)
    normed = (rows * gain_ref[...].astype(f32)).astype(bf16)
    for at, ref in enumerate((wq_ref, wk_ref, wv_ref, wg_ref)):
        out_ref[:, at * WIDTH_DEV : (at + 1) * WIDTH_DEV] = dot(normed, ref[...]).astype(bf16)
    beta = wb_ref[...].astype(f32)
    decay = wd_ref[...].astype(f32)
    small = jnp.concatenate(
        [
            jnp.where(on_first, beta[:HEADS_DEV], beta[HEADS_DEV:]),
            jnp.where(on_first, decay[:HEADS_DEV], decay[HEADS_DEV:]),
            jnp.zeros((128 - 2 * HEADS_DEV, 128), f32),
        ],
        axis=0,
    ).astype(bf16)
    extra = dot(normed, small, NT)
    lane = lax.broadcasted_iota(jnp.int32, extra.shape, 1)
    gain_mid = jnp.broadcast_to(gain_mid_ref[...].astype(f32), extra.shape)
    gain_mid = jnp.where(on_first, half_turn(gain_mid), gain_mid)
    out_ref[:, SMALL_AT:TOKENS_AT] = jnp.where(lane >= 64, gain_mid, extra).astype(bf16)


def pack(own_ref, other_ref, out_ref):
    on_first = lax.axis_index("tp") == 0
    own = own_ref[...].astype(f32)
    other = other_ref[...].astype(f32)
    low = lax.broadcasted_iota(jnp.int32, own.shape, 1) < 64
    top = jnp.where(on_first, own, half_turn(other))
    bottom = jnp.where(on_first, half_turn(other), own)
    out_ref[...] = jnp.where(low, top, bottom).astype(bf16)


def mixer(
    pieces_ref,
    state_ref,
    rate_ref,
    head_gain_ref,
    mixed_ref,
    key_ref,
    correct_ref,
    keep_ref,
    gain_ref,
):
    def total(first, last):
        parts = [pieces_ref[OWN * s : OWN * (s + 1), first:last].astype(f32) for s in range(GROUP)]
        while len(parts) > 1:
            parts = [a + b for a, b in zip(parts[::2], parts[1::2])]
        return parts[0]

    def block(s, at):
        return pieces_ref[OWN * s : OWN * (s + 1), at : at + 128].astype(f32)

    small = total(SMALL_AT, TOKENS_AT)
    tokens = [block(s, TOKENS_AT) for s in range(GROUP)]
    squares = sum(part * part for part in tokens)
    row_scale = lax.rsqrt(jnp.sum(squares, axis=1, keepdims=True) / D + norm_epsilon)
    small = small * row_scale
    row = lax.broadcasted_iota(jnp.int32, (OWN, HEAD_DIM), 0)
    lane = lax.broadcasted_iota(jnp.int32, (OWN, HEAD_DIM), 1)
    keeps = jnp.zeros((OWN, HEAD_DIM), f32)
    low = lane < 64
    for s in range(0, GROUP, 2):
        gain_ref[:, FEAT * s : FEAT * (s + 2)] = jnp.where(
            low, half_turn(block(s, SMALL_AT)), block(s + 1, SMALL_AT)
        )
        ring, at = s // RING, WIDTH_DEV + FEAT * (s % RING)
        first = jnp.where(low, tokens[s], half_turn(tokens[s + 1])).astype(bf16)
        second = jnp.where(low, half_turn(tokens[s]), tokens[s + 1]).astype(bf16)
        mixed_ref[OWN * 2 * ring : OWN * (2 * ring + 1), at : at + 128] = first
        mixed_ref[OWN * (2 * ring + 1) : OWN * (2 * ring + 2), at : at + 128] = second

    def unit(vector):
        return vector * lax.rsqrt(jnp.sum(vector * vector, axis=1, keepdims=True) + norm_epsilon)

    for h in range(HEADS_DEV):
        at = h * HEAD_DIM
        query_lin, key_lin, value_lin, gate_lin = (
            total(part * WIDTH_DEV + at, part * WIDTH_DEV + at + HEAD_DIM) * row_scale
            for part in range(4)
        )
        query = unit(silu(query_lin)) * HEAD_DIM ** (-0.5)
        key = unit(silu(key_lin))
        write_rate = 1.0 / (1.0 + jnp.exp(-small[:, h : h + 1]))
        decay = small[:, HEADS_DEV + h : HEADS_DEV + h + 1]
        softplus = jnp.maximum(decay, 0.0) + jnp.log1p(jnp.exp(-jnp.abs(decay)))
        keep = jnp.exp(-rate_ref[:, h : h + 1] * softplus)
        pair = jnp.concatenate([key, query], axis=0).astype(bf16)
        recalled = jnp.zeros((OWN, HEAD_DIM), f32)
        asked = jnp.zeros((OWN, HEAD_DIM), f32)
        for b in range(OWN):
            both = dot(pair, state_ref[b, h].astype(bf16))
            recalled = jnp.where(row == b, both[:OWN], recalled)
            asked = jnp.where(row == b, both[OWN:], asked)
        correction = write_rate * (silu(value_lin) - keep * recalled)
        readout = keep * asked + jnp.sum(key * query, axis=1, keepdims=True) * correction
        readout = readout * lax.rsqrt(
            jnp.mean(readout * readout, axis=1, keepdims=True) + norm_epsilon
        )
        mixed = (readout * head_gain_ref[...] * silu(gate_lin)).astype(bf16)
        for e in range(2 * RING):
            mixed_ref[OWN * e : OWN * (e + 1), at : at + HEAD_DIM] = mixed
        key_ref[:, at : at + HEAD_DIM] = key
        correct_ref[:, at : at + HEAD_DIM] = correction
        keeps = jnp.where(lane == h, keep, keeps)
    keep_ref[...] = keeps


def update(state_ref, key_ref, correct_ref, keep_ref, after_ref, next_ref, token_ref, made_ref, sems):
    del after_ref
    copies = []
    for b in range(OWN):
        for h in range(HEADS_DEV):
            at = h * HEAD_DIM
            key_column = jnp.broadcast_to(key_ref[b : b + 1, at : at + HEAD_DIM], (128, 128)).T
            made_ref[b, h] = (
                keep_ref[b : b + 1, h : h + 1] * state_ref[b, h]
                + key_column * correct_ref[b : b + 1, at : at + HEAD_DIM]
            )
        copies.append(pltpu.make_async_copy(made_ref.at[b], next_ref.at[b], sems.at[b]))
        copies[-1].start()
    token_ref[...] = jnp.zeros(token_ref.shape, f32)
    for copy in copies:
        copy.wait()


def updated(*operands):
    return pl.pallas_call(
        update,
        out_shape=[shape(operands[0].shape, f32), shape((8, 128), f32)],
        in_specs=[in_vmem()] * 4 + [anywhere()],
        out_specs=[pl.BlockSpec(memory_space=pltpu.HBM), in_vmem()],
        scratch_shapes=[
            pltpu.VMEM((OWN, HEADS_DEV, HEAD_DIM, HEAD_DIM), f32),
            pltpu.SemaphoreType.DMA((OWN,)),
        ],
        name="update",
        compiler_params=pltpu.CompilerParams(vmem_limit_bytes=12 * 1024 * 1024),
    )(*operands)


def preload(*refs):
    count = (len(refs) - 1) // 2
    sems = refs[-1]
    copies = [
        pltpu.make_async_copy(refs[i], refs[count + i], sems.at[i]) for i in range(count)
    ]
    for copy in copies:
        copy.start()
    for copy in copies:
        copy.wait()


def preloaded(*arrays):
    return pl.pallas_call(
        preload,
        out_shape=[shape(x.shape, x.dtype) for x in arrays],
        in_specs=[pl.BlockSpec(memory_space=pltpu.HBM)] * len(arrays),
        out_specs=[in_vmem() for _ in arrays],
        scratch_shapes=[pltpu.SemaphoreType.DMA((len(arrays),))],
        name="preload",
        compiler_params=pltpu.CompilerParams(vmem_limit_bytes=4 * 1024 * 1024),
    )(*(pltpu.with_memory_space_constraint(x, pltpu.HBM) for x in arrays))


def mix(received_ref, held_ref, next_ref, far_ref, last_ref, sent_ref):
    place = lax.axis_index("kv_1")

    def rows(core, first, last):
        return [
            received_ref[OWN * (2 * r + core) : OWN * (2 * r + core + 1), first:last].astype(f32)
            for r in range(RING)
        ]

    tokens = jnp.concatenate(rows(0, WIDTH_DEV, MIXED), axis=0)
    mixed = jnp.concatenate(rows(0, 0, WIDTH_DEV) + rows(1, 0, WIDTH_DEV), axis=0).astype(bf16)
    parts = []
    for ref in (held_ref, next_ref, far_ref, last_ref):
        both = dot(mixed, ref[...])
        parts.append(both[:SEQ_RING] + half_turn(both[SEQ_RING:]))

    def part(column):
        which = jnp.bitwise_xor(place, column)
        value = parts[0]
        for m in range(1, RING):
            value = jnp.where(which == m, parts[m], value)
        return value

    low = lax.broadcasted_iota(jnp.int32, parts[0].shape, 1) < 64
    attn = jnp.concatenate(
        [jnp.where(low, part(c), half_turn(part(c + 1))) for c in range(0, RING, 2)], axis=1
    )
    middle = (tokens + attn).astype(bf16)
    for s in range(GROUP):
        sent_ref[SEQ_RING * s : SEQ_RING * (s + 1)] = middle


def gate_up(received_ref, gain_ref, wg_ref, wu_ref, own_ref, sent_ref, middle_ref, rows_ref):
    for s in range(GROUP):
        ring, place = s // RING, s % RING
        for r in range(RING):
            rows_ref[
                SEQ_RING * r + OWN * place : SEQ_RING * r + OWN * (place + 1),
                FEAT_RING * ring : FEAT_RING * (ring + 1),
            ] = received_ref[SEQ_RING * s + OWN * r : SEQ_RING * s + OWN * (r + 1)]
    middle = rows_ref[...].astype(f32)
    normed = (middle * gain_ref[0:1]).astype(bf16)
    for at, ref in ((0, wg_ref), (HIDDEN, wu_ref)):
        value = dot(ref[...], normed, NT)
        own_ref[at : at + HIDDEN] = value
        sent_ref[at : at + HIDDEN] = value.astype(bf16)
    squares = jnp.sum(middle * middle, axis=1, keepdims=True)
    total = jnp.broadcast_to(squares, (ROWS, 128)).T[0:1]
    high, low = high_low(total)
    own_ref[BOTH:] = jnp.broadcast_to(total, (8, ROWS))
    sent_ref[BOTH:] = jnp.concatenate([high, low, jnp.zeros((6, ROWS), f32)], axis=0).astype(bf16)
    place = lax.axis_index("kv_1")
    pair = lax.axis_index("kv_0") * 2 + jnp.right_shift(place, 1)
    block = rows_ref[:, pl.ds(pl.multiple_of(pair * 128, 128), 128)].astype(f32).T
    even = jnp.bitwise_and(place, 1) == 0
    middle_ref[...] = jnp.where(even, block[:FEAT], block[FEAT:]).astype(bf16)


def down(own_ref, other_ref, w_ref, after_ref, out_ref):
    del after_ref
    squares = other_ref[BOTH:].astype(f32)
    total = own_ref[BOTH : BOTH + 1] + squares[0:1] + squares[1:2]
    scale = lax.rsqrt(total / D + norm_epsilon)
    gate = (own_ref[:HIDDEN] + other_ref[:HIDDEN].astype(f32)) * scale
    up = (own_ref[HIDDEN:BOTH] + other_ref[HIDDEN:BOTH].astype(f32)) * scale
    active = (silu(gate) * up).astype(bf16)
    out_ref[...] = dot(w_ref[...], active, TN).astype(bf16)


def finish(received_ref, middle_ref, out_ref):
    parts = [received_ref[FEAT * s : FEAT * (s + 1)].astype(f32) for s in range(GROUP)]
    while len(parts) > 1:
        parts = [a + b for a, b in zip(parts[::2], parts[1::2])]
    out_ref[...] = (middle_ref[...].astype(f32) + parts[0]).astype(bf16)


def from_other_core(array):
    return lax.ppermute(array, "tp", [(0, 1), (1, 0)])


def over(array, axes, members):
    tiles = array.reshape(members, array.shape[0] // members, array.shape[1])
    return lax.all_to_all(tiles, axes, 0, 0, tiled=True).reshape(array.shape)


def from_ring(array, flip):
    return lax.ppermute(array, "kv_1", [(i, i ^ flip) for i in range(RING)])


def layer(
    tokens,
    delta_state,
    gain_in,
    w_query,
    w_key,
    w_value,
    w_out_gate,
    w_beta,
    w_decay,
    decay_rate,
    head_gain,
    w_mix,
    gain_mid,
    w_gate,
    w_up,
    w_down,
):
    v, a = in_vmem(), anywhere()
    own_tokens = tokens.T
    other_tokens = from_other_core(own_tokens)
    other_mix = from_other_core(w_mix)
    *loaded, own_mix = preloaded(
        own_tokens,
        gain_in.reshape(1, 128),
        gain_mid.reshape(1, 128),
        w_query,
        w_key,
        w_value,
        w_out_gate,
        w_beta.T,
        w_decay.T,
        w_mix,
    )
    held = kernel(pack, shape(w_mix.shape, bf16), [v] * 2)(own_mix, other_mix)
    near = from_ring(held, 1)
    opposite = from_ring(held, 2)
    far = from_ring(held, 3)
    summand = kernel(project, shape((ROWS, PIECE), bf16), [v] * 10 + [a])(
        *loaded, other_tokens, held
    )
    pieces = over(summand, KV, GROUP)
    mixed, key, correction, keep, gains = kernel(
        mixer,
        [
            shape((2 * RING * OWN, MIXED), bf16),
            shape((OWN, WIDTH_DEV), f32),
            shape((OWN, WIDTH_DEV), f32),
            shape((OWN, HEAD_DIM), f32),
            shape((OWN, GROUP * FEAT), f32),
        ],
        [v] * 4,
    )(pieces, delta_state, decay_rate.reshape(1, HEADS_DEV), head_gain.reshape(1, HEAD_DIM))
    mixed_rows = over(mixed, ("kv_0", "tp"), 2 * RING)
    sent = kernel(mix, shape((GROUP * SEQ_RING, FEAT_RING), bf16), [v] * 5)(
        mixed_rows, held, near, opposite, far
    )
    received = over(sent, KV, GROUP)
    own_sum, sent_sum, middle = pl.pallas_call(
        gate_up,
        out_shape=[
            shape((BOTH + 8, ROWS), f32),
            shape((BOTH + 8, ROWS), bf16),
            shape((FEAT, ROWS), bf16),
        ],
        in_specs=[v] * 4,
        out_specs=[v] * 3,
        scratch_shapes=[pltpu.VMEM((ROWS, GROUP * FEAT), bf16)],
        name="gate_up",
        compiler_params=pltpu.CompilerParams(vmem_limit_bytes=12 * 1024 * 1024),
    )(received, gains, w_gate.T, w_up.T)
    next_state, token = updated(delta_state, key, correction, keep, received)
    down_local = kernel(down, shape((GROUP * FEAT, ROWS), bf16), [v, v, v, a])(
        own_sum, from_other_core(sent_sum), w_down, token
    )
    layer_out = kernel(finish, shape((FEAT, ROWS), bf16), [v] * 2)(
        over(down_local, KV, GROUP), middle
    )
    return (layer_out.T, next_state)


def solution(mesh):
    split = Mesh(
        mesh.devices.reshape(mesh.shape["dp"], 4, 4, mesh.shape["tp"]), ("dp", "kv_0", "kv_1", "tp")
    )
    in_specs = (
        P("dp", KV_TP),
        P(DP_KV, "tp", None, None),
        P(KV),
        P(KV, "tp"),
        P(KV, "tp"),
        P(KV, "tp"),
        P(KV, "tp"),
        P(KV, None),
        P(KV, None),
        P("tp"),
        P(),
        P("tp", KV),
        P(KV),
        P("tp", KV),
        P("tp", KV),
        P(KV, "tp"),
    )
    out_specs = (P("dp", KV_TP), P(DP_KV, "tp", None, None))
    return jax.shard_map(layer, mesh=split, in_specs=in_specs, out_specs=out_specs, check_vma=False)
```

time: 65 us -> 70.5 us (1.085)
  blocking collectives: 51.7 us -> 21.6 us
  starting transfers between devices: 5.55 us -> 21.5 us
  waiting for transfers between devices: 0.01 us -> 12.4 us
  local copies, waits for them, and re-layouts: 0.05 us -> 5.67 us
  Pallas kernels: 6.61 us -> 7.94 us
    all_to_all x4 -> x2, blocking collectives: 51.7 us -> 21.6 us  [over(): return lax.all_to_all(tiles, axes, 0, 0, tiled=True).reshape(array.shape)]
    all_to_all x0 -> x2, starting transfers between devices: none -> 14.2 us  [over(): return lax.all_to_all(tiles, axes, 0, 0, tiled=True).reshape(array.shape)]
    all_to_all x0 -> x2, waiting for transfers between devices: none -> 12.4 us  [over(): return lax.all_to_all(tiles, axes, 0, 0, tiled=True).reshape(array.shape)]
    unnamed x16 -> x26, local copies, waits for them, and re-layouts: 0.05 us -> 5.67 us
    ppermute x0 -> x3, starting transfers between devices: none -> 3.94 us  [from_ring(): return lax.ppermute(array, 'kv_1', [(i, i ^ flip) for i in range(RING)])]
    ppermute x3, starting transfers between devices: 5.55 us -> 3.3 us  [from_other_core(): return lax.ppermute(array, 'tp', [(0, 1), (1, 0)])]
    pallas_call x9 -> x8, Pallas kernels: 5.41 us -> 6.63 us  [the longest x1 1.56 us: updated(): pl.pallas_call(update, out_shape=[shape(operands[0].shape, f32), shape((8...]
  transfers between devices with their start and end apart: 3 -> 8, of which waited for: 0 -> 2; matrix products, arithmetic and copies ran while one was open for 0% -> 0% of each run, Pallas kernels for 5% -> 5%
where the time goes in v4:
time: 70.5 us; the launch traced here: 69.9 us
  blocking collectives  21.6 us (31%)
  starting transfers between devices  21.5 us (30%)
  waiting for transfers between devices  12.4 us (18%)
  Pallas kernels  7.94 us (11%)
  local copies, waits for them, and re-layouts  5.67 us (8%)
  between operations  0.75 us (1%)
    all_to_all x2, blocking collectives, over(): return lax.all_to_all(tiles, axes, 0, 0, tiled=True).reshape(array.shape)  21.6 us
    all_to_all x2, starting transfers between devices, over(): return lax.all_to_all(tiles, axes, 0, 0, tiled=True).reshape(array.shape)  14.2 us
    all_to_all x2, waiting for transfers between devices, over(): return lax.all_to_all(tiles, axes, 0, 0, tiled=True).reshape(array.shape)  12.4 us
    unnamed x26, local copies, waits for them, and re-layouts  5.67 us
    ppermute x3, starting transfers between devices, from_ring(): return lax.ppermute(array, 'kv_1', [(i, i ^ flip) for i in range(RING)])  3.94 us
    ppermute x3, starting transfers between devices, from_other_core(): return lax.ppermute(array, 'tp', [(0, 1), (1, 0)])  3.3 us
    pallas_call x1, Pallas kernels, updated(): pl.pallas_call(update, out_shape=[shape(operands[0].shape, f32), shape((8...  1.56 us
    pallas_call x1, Pallas kernels, layer(): kernel(mix, shape((GROUP * SEQ_RING, FEAT_RING), bf16), [v] * 5)  1.48 us
  transfers between devices with their start and end apart: 8, of which 2 were waited for; matrix products, arithmetic and copies ran while one was open for 0% of the time, Pallas kernels for 5%

profile of v4, /device:TPU:1, one launch (start us, length us, event | category | flops | bytes accessed | tf_op | source)
XLA Modules:
  0.0 69.9 jit_solution(2534999007904925068)
XLA Ops:
  0.6 1.5 %collective-permute-start.1 = (bf16[512,128]{1,0:T(8,128)(2,1)}, bf16[512,128]{1,0:T(8,128)(2,1)S(1)}, u32[]{:S(2)}, u32[]{:S(2)}) collective-permute-start(bf16[512,128]{1,0:T(8,128)(2,1)} %refs_9_.1), channel_id=1, source_target_pairs={{0,1},{1,0},{2,3},{3,2},{4,5},{5,4},{6,7},{7,6},{8,9},{9,8},{10,11... | collective-permute-start | bytes 393224 | tf_op jit(solution)/shard_map/ppermute | solution.py:330
  2.2 1.3 %preload.1 = (bf16[64,128]{1,0:T(8,128)(2,1)S(1)}, bf16[1,128]{1,0:T(2,128)(2,1)S(1)}, bf16[1,128]{1,0:T(2,128)(2,1)S(1)}, bf16[128,512]{1,0:T(8,128)(2,1)S(1)},...) custom-call(bf16[64,128]{1,0:T(8,128)(2,1)} %bitcast.32, ...), custom_call_target="tpu_custom_call" | custom-call | tf_op jit(solution)/shard_map/preload/pallas_call | solution.py:242
  3.7 1.2 %shard_map.168 = bf16[128,2304]{1,0:T(8,128)(2,1)} custom-call(bf16[64,128]{1,0:T(8,128)(2,1)S(1)} %get-tuple-element.22.own_ref, bf16[1,128]{1,0:T(2,128)(2,1)S(1)} %get-tuple-element.23.gain_ref, bf16[1,128]{1,0:T(2,128)(2,1)S(1)} %get-tuple-element.24.gain_mid_ref, bf16[128,512]{1,0:T(8,128)(2,1)S(1)} %get-tuple-element.25.wq_ref, ...), custom_call_target="tpu_custom_call" | custom-call | tf_op jit(solution)/shard_map/pallas_call | solution.py:380
  4.8 7.9 %all-to-all-start = ((bf16[16,8,2304]{2,1,0:T(8,128)(2,1)}), bf16[16,8,2304]{2,1,0:T(8,128)(2,1)S(1)}, u32[]{:S(2)}, u32[]{:S(2)}) async-start(bf16[16,8,2304]{2,1,0:T(8,128)(2,1)} %bitcast.5), calls=%async_computation | async-start | bytes 1179648 | tf_op jit(solution)/shard_map/all_to_all | solution.py:335
  12.7 1.4 %collective-permute-start.2 = (bf16[512,128]{1,0:T(8,128)(2,1)S(1)}, bf16[512,128]{1,0:T(8,128)(2,1)}, u32[]{:S(2)}, u32[]{:S(2)}) collective-permute-start(bf16[512,128]{1,0:T(8,128)(2,1)S(1)} %shard_map.167.after_ref.held_ref), channel_id=1, source_target_pairs={{0,2},{2,0},{4,6},{6,4},{1,3},{3,1},{5,7},{7,5},{8,10},{10,8},{12,... | collective-permute-start | bytes 393224 | tf_op jit(solution)/shard_map/ppermute | solution.py:339
  14.1 2.4 %collective-permute-start.3 = (bf16[512,128]{1,0:T(8,128)(2,1)S(1)}, bf16[512,128]{1,0:T(8,128)(2,1)}, u32[]{:S(2)}, u32[]{:S(2)}) collective-permute-start(bf16[512,128]{1,0:T(8,128)(2,1)S(1)} %shard_map.167.after_ref.held_ref), channel_id=1, source_target_pairs={{0,4},{2,6},{4,0},{6,2},{1,5},{3,7},{5,1},{7,3},{8,12},{10,14},{12... | collective-permute-start | bytes 393224 | tf_op jit(solution)/shard_map/ppermute | solution.py:339
  16.7 7.4 %all-to-all-done = bf16[16,8,2304]{2,1,0:T(8,128)(2,1)S(1)} async-done(((bf16[16,8,2304]{2,1,0:T(8,128)(2,1)}), bf16[16,8,2304]{2,1,0:T(8,128)(2,1)S(1)}, u32[]{:S(2)}, u32[]{:S(2)}) %all-to-all-start) | async-done | bytes 589856 | tf_op jit(solution)/shard_map/all_to_all | solution.py:335
  24.1 0.7 copy-done.11
  24.8 0.7 copy-done.12
  25.4 0.6 shard_map.169
  26.1 0.7 copy-done.4
  26.7 0.6 copy-done.5
  27.3 0.6 copy-done.7
  27.9 0.6 copy-done.9
  28.5 6.4 %all-to-all-start.1 = ((bf16[8,8,768]{2,1,0:T(8,128)(2,1)}), bf16[8,8,768]{2,1,0:T(8,128)(2,1)S(1)}, u32[]{:S(2)}, u32[]{:S(2)}) async-start(bf16[8,8,768]{2,1,0:T(8,128)(2,1)} %bitcast.27), calls=%async_computation.1 | async-start | bytes 196608 | tf_op jit(solution)/shard_map/all_to_all | solution.py:335
  34.9 5.0 %all-to-all-done.1 = bf16[8,8,768]{2,1,0:T(8,128)(2,1)S(1)} async-done(((bf16[8,8,768]{2,1,0:T(8,128)(2,1)}), bf16[8,8,768]{2,1,0:T(8,128)(2,1)S(1)}, u32[]{:S(2)}, u32[]{:S(2)}) %all-to-all-start.1) | async-done | bytes 98336 | tf_op jit(solution)/shard_map/all_to_all | solution.py:335
  39.9 1.5 %shard_map.170 = bf16[512,256]{1,0:T(8,128)(2,1)S(1)} custom-call(bf16[64,768]{1,0:T(8,128)(2,1)S(1)} %bitcast.26, bf16[512,128]{1,0:T(8,128)(2,1)S(1)} %shard_map.167.after_ref.held_ref, bf16[512,128]{1,0:T(8,128)(2,1)} %collective-permute-done.2.next_ref, bf16[512,128]{1,0:T(8,128)(2,1)} %collective-permute-done.3.far_ref, ...), custom_call_target="tpu_custom_call" | custom-call | tf_op jit(solution)/shard_map/pallas_call | solution.py:396
  41.4 10.6 %all_to_all.20 = bf16[16,32,256]{2,1,0:T(8,128)(2,1)S(1)} all-to-all(bf16[16,32,256]{2,1,0:T(8,128)(2,1)S(1)} %bitcast.21), channel_id=1, replica_groups=mesh['dp'=4,'kv_0'=4,'kv_1'=4,'tp'=2] {'kv_0','kv_1'}, dimensions={0} | all-to-all | bytes 524288 | tf_op jit(solution)/shard_map/all_to_all | solution.py:335
  52.0 1.1 %copy-done.2 = bf16[1024,352]{0,1:T(8,128)(2,1)S(1)} copy-done((bf16[1024,352]{0,1:T(8,128)(2,1)S(1)}, bf16[1024,352]{0,1:T(8,128)(2,1)}, u32[]{:S(2)}) %copy-start.2) | copy-done | bytes 720920
  53.1 0.8 %copy-done.6 = f32[8,1024]{1,0:T(8,128)S(1)} copy-done((f32[8,1024]{1,0:T(8,128)S(1)}, f32[8,1024]{1,0:T(8,128)}, u32[]{:S(2)}) %copy-start.6) | copy-done | bytes 32792
  54.4 1.7 %collective-permute-start.5 = (bf16[712,128]{1,0:T(8,128)(2,1)S(1)}, bf16[712,128]{1,0:T(8,128)(2,1)S(1)}, u32[]{:S(2)}, u32[]{:S(2)}) collective-permute-start(bf16[712,128]{1,0:T(8,128)(2,1)S(1)} %get-tuple-element.35), channel_id=1, source_target_pairs={{0,1},{1,0},{2,3},{3,2},{4,5},{5,4},{6,7},{7,6},{8,9},{9,8},{10,11... | collective-permute-start | bytes 546824 | tf_op jit(solution)/shard_map/ppermute | solution.py:330
  56.1 1.6 %update.1 = (f32[8,4,128,128]{3,2,1,0:T(8,128)}, f32[8,128]{1,0:T(8,128)S(1)}) custom-call(f32[8,4,128,128]{3,2,1,0:T(8,128)S(1)} %copy-done, f32[8,512]{1,0:T(8,128)S(1)} %get-tuple-element.36.key_ref, f32[8,512]{1,0:T(8,128)S(1)} %copy-done.8, f32[8,128]{1,0:T(8,128)S(1)} %copy-done.10, bf16[512,256]{1,0:T(8,128)(2,1)S(1)} %bitcast.20), custom_call_target="tpu_custom_call" | custom-call | tf_op jit(solution)/shard_map/update/pallas_call | solution.py:215
  58.2 11.1 %all_to_all.21 = bf16[16,64,128]{2,1,0:T(8,128)(2,1)S(1)} all-to-all(bf16[16,64,128]{2,1,0:T(8,128)(2,1)S(1)} %bitcast.23), channel_id=1, replica_groups=mesh['dp'=4,'kv_0'=4,'kv_1'=4,'tp'=2] {'kv_0','kv_1'}, dimensions={0} | all-to-all | bytes 524288 | tf_op jit(solution)/shard_map/all_to_all | solution.py:335
  69.3 0.6 shard_map.172
  (29 shorter events, 1.4 us)
Async XLA Ops:
  0.6 23.5 %copy-start = (f32[8,4,128,128]{3,2,1,0:T(8,128)S(1)}, f32[8,4,128,128]{3,2,1,0:T(8,128)}, u32[]{:S(2)}) copy-start(f32[8,4,128,128]{3,2,1,0:T(8,128)} %state_ref.3) | copy-start | bytes 6291460
  0.6 2.9 %collective-permute-start.1 = (bf16[512,128]{1,0:T(8,128)(2,1)}, bf16[512,128]{1,0:T(8,128)(2,1)S(1)}, u32[]{:S(2)}, u32[]{:S(2)}) collective-permute-start(bf16[512,128]{1,0:T(8,128)(2,1)} %refs_9_.1), channel_id=1, source_target_pairs={{0,1},{1,0},{2,3},{3,2},{4,5},{5,4},{6,7},{7,6},{8,9},{9,8},{10,11... | collective-permute-start | bytes 393224 | tf_op jit(solution)/shard_map/ppermute | solution.py:330
  2.1 1.6 %collective-permute-start = (bf16[64,128]{1,0:T(8,128)(2,1)}, bf16[64,128]{1,0:T(8,128)(2,1)S(1)}, u32[]{:S(2)}, u32[]{:S(2)}) collective-permute-start(bf16[64,128]{1,0:T(8,128)(2,1)} %bitcast.31), channel_id=1, source_target_pairs={{0,1},{1,0},{2,3},{3,2},{4,5},{5,4},{6,7},{7,6},{8,9},{9,8},{10,11... | collective-permute-start | bytes 49160 | tf_op jit(solution)/shard_map/ppermute | solution.py:330
  4.8 19.3 %all-to-all-start = ((bf16[16,8,2304]{2,1,0:T(8,128)(2,1)}), bf16[16,8,2304]{2,1,0:T(8,128)(2,1)S(1)}, u32[]{:S(2)}, u32[]{:S(2)}) async-start(bf16[16,8,2304]{2,1,0:T(8,128)(2,1)} %bitcast.5), calls=%async_computation | async-start | bytes 1179648 | tf_op jit(solution)/shard_map/all_to_all | solution.py:335
  12.7 22.2 %collective-permute-start.2 = (bf16[512,128]{1,0:T(8,128)(2,1)S(1)}, bf16[512,128]{1,0:T(8,128)(2,1)}, u32[]{:S(2)}, u32[]{:S(2)}) collective-permute-start(bf16[512,128]{1,0:T(8,128)(2,1)S(1)} %shard_map.167.after_ref.held_ref), channel_id=1, source_target_pairs={{0,2},{2,0},{4,6},{6,4},{1,3},{3,1},{5,7},{7,5},{8,10},{10,8},{12,... | collective-permute-start | bytes 393224 | tf_op jit(solution)/shard_map/ppermute | solution.py:339
  14.1 20.8 %collective-permute-start.3 = (bf16[512,128]{1,0:T(8,128)(2,1)S(1)}, bf16[512,128]{1,0:T(8,128)(2,1)}, u32[]{:S(2)}, u32[]{:S(2)}) collective-permute-start(bf16[512,128]{1,0:T(8,128)(2,1)S(1)} %shard_map.167.after_ref.held_ref), channel_id=1, source_target_pairs={{0,4},{2,6},{4,0},{6,2},{1,5},{3,7},{5,1},{7,3},{8,12},{10,14},{12... | collective-permute-start | bytes 393224 | tf_op jit(solution)/shard_map/ppermute | solution.py:339
  16.5 18.4 %collective-permute-start.4 = (bf16[512,128]{1,0:T(8,128)(2,1)S(1)}, bf16[512,128]{1,0:T(8,128)(2,1)}, u32[]{:S(2)}, u32[]{:S(2)}) collective-permute-start(bf16[512,128]{1,0:T(8,128)(2,1)S(1)} %shard_map.167.after_ref.held_ref), channel_id=1, source_target_pairs={{0,6},{2,4},{4,2},{6,0},{1,7},{3,5},{5,3},{7,1},{8,14},{10,12},{12... | collective-permute-start | bytes 393224 | tf_op jit(solution)/shard_map/ppermute | solution.py:339
  24.1 0.7 copy-start.11
  24.8 0.7 copy-start.12
  25.4 26.5 %copy-start.1 = (bf16[1024,352]{0,1:T(8,128)(2,1)S(1)}, bf16[1024,352]{0,1:T(8,128)(2,1)}, u32[]{:S(2)}) copy-start(bf16[1024,352]{0,1:T(8,128)(2,1)} %param.29) | copy-start | bytes 2162692
  26.1 0.7 copy-start.4
  26.7 0.6 copy-start.5
  27.3 0.6 copy-start.7
  27.9 0.6 copy-start.9
  28.5 27.6 %copy-start.8 = (f32[8,512]{1,0:T(8,128)S(1)}, f32[8,512]{1,0:T(8,128)}, u32[]{:S(2)}) copy-start(f32[8,512]{1,0:T(8,128)} %copy-done.7) | copy-start | bytes 49156
  28.5 27.6 %copy-start.10 = (f32[8,128]{1,0:T(8,128)S(1)}, f32[8,128]{1,0:T(8,128)}, u32[]{:S(2)}) copy-start(f32[8,128]{1,0:T(8,128)} %copy-done.9) | copy-start | bytes 12292
  28.5 11.4 %all-to-all-start.1 = ((bf16[8,8,768]{2,1,0:T(8,128)(2,1)}), bf16[8,8,768]{2,1,0:T(8,128)(2,1)S(1)}, u32[]{:S(2)}, u32[]{:S(2)}) async-start(bf16[8,8,768]{2,1,0:T(8,128)(2,1)} %bitcast.27), calls=%async_computation.1 | async-start | bytes 196608 | tf_op jit(solution)/shard_map/all_to_all | solution.py:335
  39.9 17.8 %copy-start.3 = (bf16[352,1024]{1,0:T(8,128)(2,1)S(1)}, bf16[352,1024]{1,0:T(8,128)(2,1)}, u32[]{:S(2)}) copy-start(bf16[352,1024]{1,0:T(8,128)(2,1)} %w_ref.1) | copy-start | bytes 2162692
  52.0 1.1 %copy-start.2 = (bf16[1024,352]{0,1:T(8,128)(2,1)S(1)}, bf16[1024,352]{0,1:T(8,128)(2,1)}, u32[]{:S(2)}) copy-start(bf16[1024,352]{0,1:T(8,128)(2,1)} %param.30) | copy-start | bytes 2162692
  53.1 0.8 %copy-start.6 = (f32[8,1024]{1,0:T(8,128)S(1)}, f32[8,1024]{1,0:T(8,128)}, u32[]{:S(2)}) copy-start(f32[8,1024]{1,0:T(8,128)} %copy-done.5) | copy-start | bytes 98308
  54.4 3.3 %collective-permute-start.5 = (bf16[712,128]{1,0:T(8,128)(2,1)S(1)}, bf16[712,128]{1,0:T(8,128)(2,1)S(1)}, u32[]{:S(2)}, u32[]{:S(2)}) collective-permute-start(bf16[712,128]{1,0:T(8,128)(2,1)S(1)} %get-tuple-element.35), channel_id=1, source_target_pairs={{0,1},{1,0},{2,3},{3,2},{4,5},{5,4},{6,7},{7,6},{8,9},{9,8},{10,11... | collective-permute-start | bytes 546824 | tf_op jit(solution)/shard_map/ppermute | solution.py:330

commit v5 on v4

--- a/solution.py
+++ b/solution.py
@@ -250,21 +250,46 @@
     )(*(pltpu.with_memory_space_constraint(x, pltpu.HBM) for x in arrays))
 
 
-def mix(received_ref, held_ref, next_ref, far_ref, last_ref, sent_ref):
+def note(after_ref, out_ref):
+    del after_ref
+    out_ref[...] = jnp.zeros(out_ref.shape, f32)
+
+
+def join(held_ref, near_ref, after_ref, out_ref):
+    del after_ref
+    out_ref[:WIDTH_DEV] = held_ref[...]
+    out_ref[WIDTH_DEV:] = near_ref[...]
+
+
+def ring_rows(received_ref, core, first, last):
+    return [
+        received_ref[OWN * (2 * r + core) : OWN * (2 * r + core + 1), first:last].astype(f32)
+        for r in range(RING)
+    ]
+
+
+def ring_parts(received_ref, joined_ref):
+    mixed = jnp.concatenate(
+        ring_rows(received_ref, 0, 0, WIDTH_DEV) + ring_rows(received_ref, 1, 0, WIDTH_DEV), axis=0
+    ).astype(bf16)
+    parts = []
+    for at in (0, WIDTH_DEV):
+        both = dot(mixed, joined_ref[at : at + WIDTH_DEV])
+        parts.append(both[:SEQ_RING] + half_turn(both[SEQ_RING:]))
+    return parts
+
+
+def mix_near(received_ref, joined_ref, part_ref):
+    own, third = ring_parts(received_ref, joined_ref)
+    part_ref[:SEQ_RING] = own
+    part_ref[SEQ_RING:] = third
+
+
+def mix(received_ref, far_ref, part_ref, sent_ref):
     place = lax.axis_index("kv_1")
-
-    def rows(core, first, last):
-        return [
-            received_ref[OWN * (2 * r + core) : OWN * (2 * r + core + 1), first:last].astype(f32)
-            for r in range(RING)
-        ]
-
-    tokens = jnp.concatenate(rows(0, WIDTH_DEV, MIXED), axis=0)
-    mixed = jnp.concatenate(rows(0, 0, WIDTH_DEV) + rows(1, 0, WIDTH_DEV), axis=0).astype(bf16)
-    parts = []
-    for ref in (held_ref, next_ref, far_ref, last_ref):
-        both = dot(mixed, ref[...])
-        parts.append(both[:SEQ_RING] + half_turn(both[SEQ_RING:]))
+    tokens = jnp.concatenate(ring_rows(received_ref, 0, WIDTH_DEV, MIXED), axis=0)
+    first, second = ring_parts(received_ref, far_ref)
+    parts = [part_ref[:SEQ_RING], first, second, part_ref[SEQ_RING:]]
 
     def part(column):
         which = jnp.bitwise_xor(place, column)
@@ -374,13 +399,14 @@
         w_mix,
     )
     held = kernel(pack, shape(w_mix.shape, bf16), [v] * 2)(own_mix, other_mix)
-    near = from_ring(held, 1)
-    opposite = from_ring(held, 2)
-    far = from_ring(held, 3)
+    near = from_ring(held, 3)
     summand = kernel(project, shape((ROWS, PIECE), bf16), [v] * 10 + [a])(
         *loaded, other_tokens, held
     )
     pieces = over(summand, KV, GROUP)
+    mark = kernel(note, shape((8, 128), f32), [a])(pieces)
+    joined = kernel(join, shape((2 * WIDTH_DEV, 128), bf16), [v, v, a])(held, near, mark)
+    far = from_ring(joined, 1)
     mixed, key, correction, keep, gains = kernel(
         mixer,
         [
@@ -393,8 +419,9 @@
         [v] * 4,
     )(pieces, delta_state, decay_rate.reshape(1, HEADS_DEV), head_gain.reshape(1, HEAD_DIM))
     mixed_rows = over(mixed, ("kv_0", "tp"), 2 * RING)
-    sent = kernel(mix, shape((GROUP * SEQ_RING, FEAT_RING), bf16), [v] * 5)(
-        mixed_rows, held, near, opposite, far
+    near_part = kernel(mix_near, shape((2 * SEQ_RING, 128), f32), [v] * 2)(mixed_rows, joined)
+    sent = kernel(mix, shape((GROUP * SEQ_RING, FEAT_RING), bf16), [v] * 3)(
+        mixed_rows, far, near_part
     )
     received = over(sent, KV, GROUP)
     own_sum, sent_sum, middle = pl.pallas_call(

time: 70.5 us -> 64.8 us (0.919)
  blocking collectives: 21.6 us -> 32 us
  starting transfers between devices: 21.5 us -> 14.4 us
  local copies, waits for them, and re-layouts: 5.67 us -> 0.04 us
  waiting for transfers between devices: 12.4 us -> 10.2 us
  Pallas kernels: 7.94 us -> 7.07 us
    all_to_all x2 -> x3, blocking collectives: 21.6 us -> 32 us  [over(): return lax.all_to_all(tiles, axes, 0, 0, tiled=True).reshape(array.shape)]
    all_to_all x2 -> x1, starting transfers between devices: 14.2 us -> 7.88 us  [over(): return lax.all_to_all(tiles, axes, 0, 0, tiled=True).reshape(array.shape)]
    unnamed x26 -> x12, local copies, waits for them, and re-layouts: 5.67 us -> 0.04 us
    all_to_all x2 -> x1, waiting for transfers between devices: 12.4 us -> 8.81 us  [over(): return lax.all_to_all(tiles, axes, 0, 0, tiled=True).reshape(array.shape)]
    ppermute x3 -> x2, waiting for transfers between devices: 0.01 us -> 1.38 us  [from_ring(): return lax.ppermute(array, 'kv_1', [(i, i ^ flip) for i in range(RING)])]
    ppermute x3 -> x2, starting transfers between devices: 3.94 us -> 2.66 us  [from_ring(): return lax.ppermute(array, 'kv_1', [(i, i ^ flip) for i in range(RING)])]
    pallas_call x1 -> x4, Pallas kernels: 1.48 us -> 0.59 us  [the longest x1 0.33 us: layer(): kernel(mix, shape((GROUP * SEQ_RING, FEAT_RING), bf16), [v] * 3)]
  transfers between devices with their start and end apart: 8 -> 6, of which waited for: 2 -> 2; matrix products, arithmetic and copies ran while one was open for 0% -> 0% of each run, Pallas kernels for 5% -> 6%
where the time goes in v5:
time: 64.8 us; the launch traced here: 64.5 us
  blocking collectives  32 us (49%)
  starting transfers between devices  14.4 us (22%)
  waiting for transfers between devices  10.2 us (16%)
  Pallas kernels  7.07 us (11%)
  between operations  0.8 us (1%)
    all_to_all x3, blocking collectives, over(): return lax.all_to_all(tiles, axes, 0, 0, tiled=True).reshape(array.shape)  32 us
    all_to_all x1, waiting for transfers between devices, over(): return lax.all_to_all(tiles, axes, 0, 0, tiled=True).reshape(array.shape)  8.81 us
    all_to_all x1, starting transfers between devices, over(): return lax.all_to_all(tiles, axes, 0, 0, tiled=True).reshape(array.shape)  7.88 us
    ppermute x3, starting transfers between devices, from_other_core(): return lax.ppermute(array, 'tp', [(0, 1), (1, 0)])  3.87 us
    ppermute x2, starting transfers between devices, from_ring(): return lax.ppermute(array, 'kv_1', [(i, i ^ flip) for i in range(RING)])  2.66 us
    pallas_call x1, Pallas kernels, updated(): pl.pallas_call(update, out_shape=[shape(operands[0].shape, f32), shape((8...  1.56 us
    ppermute x2, waiting for transfers between devices, from_ring(): return lax.ppermute(array, 'kv_1', [(i, i ^ flip) for i in range(RING)])  1.38 us
    pallas_call x1, Pallas kernels, preloaded(): pl.pallas_call(preload, out_shape=[shape(x.shape, x.dtype) for x in array...  1.31 us
  transfers between devices with their start and end apart: 6, of which 2 were waited for; matrix products, arithmetic and copies ran while one was open for 0% of the time, Pallas kernels for 6%

profile of v5, /device:TPU:1, one launch (start us, length us, event | category | flops | bytes accessed | tf_op | source)
XLA Modules:
  0.0 64.5 jit_solution(4354825136021908684)
XLA Ops:
  0.6 1.5 %collective-permute-start.1 = (bf16[512,128]{1,0:T(8,128)(2,1)}, bf16[512,128]{1,0:T(8,128)(2,1)S(1)}, u32[]{:S(2)}, u32[]{:S(2)}) collective-permute-start(bf16[512,128]{1,0:T(8,128)(2,1)} %refs_9_.1), channel_id=1, source_target_pairs={{0,1},{1,0},{2,3},{3,2},{4,5},{5,4},{6,7},{7,6},{8,9},{9,8},{10,11... | collective-permute-start | bytes 393224 | tf_op jit(solution)/shard_map/ppermute | solution.py:355
  2.1 0.1 collective-permute-start
  2.2 1.3 %preload.1 = (bf16[64,128]{1,0:T(8,128)(2,1)S(1)}, bf16[1,128]{1,0:T(2,128)(2,1)S(1)}, bf16[1,128]{1,0:T(2,128)(2,1)S(1)}, bf16[128,512]{1,0:T(8,128)(2,1)S(1)},...) custom-call(bf16[64,128]{1,0:T(8,128)(2,1)} %bitcast.34, ...), custom_call_target="tpu_custom_call" | custom-call | tf_op jit(solution)/shard_map/preload/pallas_call | solution.py:242
  3.5 0.0 copy-start
  3.5 0.0 copy-start.4
  3.5 0.0 copy-start.5
  3.6 0.1 shard_map.167.after_ref.held_ref
  3.7 1.2 %shard_map.168 = bf16[128,2304]{1,0:T(8,128)(2,1)} custom-call(bf16[64,128]{1,0:T(8,128)(2,1)S(1)} %get-tuple-element.22.own_ref, bf16[1,128]{1,0:T(2,128)(2,1)S(1)} %get-tuple-element.23.gain_ref, bf16[1,128]{1,0:T(2,128)(2,1)S(1)} %get-tuple-element.24.gain_mid_ref, bf16[128,512]{1,0:T(8,128)(2,1)S(1)} %get-tuple-element.25.wq_ref, ...), custom_call_target="tpu_custom_call" | custom-call | tf_op jit(solution)/shard_map/pallas_call | solution.py:403
  4.9 7.9 %all-to-all-start = ((bf16[16,8,2304]{2,1,0:T(8,128)(2,1)}), bf16[16,8,2304]{2,1,0:T(8,128)(2,1)S(1)}, u32[]{:S(2)}, u32[]{:S(2)}) async-start(bf16[16,8,2304]{2,1,0:T(8,128)(2,1)} %bitcast.5), calls=%async_computation | async-start | bytes 1179648 | tf_op jit(solution)/shard_map/all_to_all | solution.py:360
  12.8 2.6 %collective-permute-start.2 = (bf16[512,128]{1,0:T(8,128)(2,1)S(1)}, bf16[512,128]{1,0:T(8,128)(2,1)S(1)}, u32[]{:S(2)}, u32[]{:S(2)}) collective-permute-start(bf16[512,128]{1,0:T(8,128)(2,1)S(1)} %shard_map.167.after_ref.held_ref), channel_id=1, source_target_pairs={{0,6},{2,4},{4,2},{6,0},{1,7},{3,5},{5,3},{7,1},{8,14},{10,12},{12... | collective-permute-start | bytes 393224 | tf_op jit(solution)/shard_map/ppermute | solution.py:364
  15.3 8.8 %all-to-all-done = bf16[16,8,2304]{2,1,0:T(8,128)(2,1)S(1)} async-done(((bf16[16,8,2304]{2,1,0:T(8,128)(2,1)}), bf16[16,8,2304]{2,1,0:T(8,128)(2,1)S(1)}, u32[]{:S(2)}, u32[]{:S(2)}) %all-to-all-start) | async-done | bytes 589856 | tf_op jit(solution)/shard_map/all_to_all | solution.py:360
  24.1 1.4 %collective-permute-done.2.near_ref = bf16[512,128]{1,0:T(8,128)(2,1)S(1)} collective-permute-done((bf16[512,128]{1,0:T(8,128)(2,1)S(1)}, bf16[512,128]{1,0:T(8,128)(2,1)S(1)}, u32[]{:S(2)}, u32[]{:S(2)}) %collective-permute-start.2) | collective-permute-done | bytes 131104 | tf_op jit(solution)/shard_map/ppermute | solution.py:364
  25.5 0.1 collective-permute-start.3
  25.7 0.6 %shard_map.169 = (bf16[64,768]{1,0:T(8,128)(2,1)S(1)}, f32[8,512]{1,0:T(8,128)S(1)}, f32[8,512]{1,0:T(8,128)S(1)}, f32[8,128]{1,0:T(8,128)S(1)}, f32[8,1024]{1,0:T(8,128)S(1)}) custom-call(bf16[128,2304]{1,0:T(8,128)(2,1)S(1)} %bitcast.19, f32[8,4,128,128]{3,2,1,0:T(8,128)S(1)} %copy-done, f32[1,4]{1,0:T(1,128)S(1)} %bitcast.30, f32[1,128]{1,0:T(1,128)S(1)} %bitcast.31), custom_call_target="tpu_custom_call" | custom-call | tf_op jit(solution)/shard_map/pallas_call | solution.py:410
  26.3 10.0 %all_to_all.20 = bf16[8,8,768]{2,1,0:T(8,128)(2,1)S(1)} all-to-all(bf16[8,8,768]{2,1,0:T(8,128)(2,1)S(1)} %bitcast.29), channel_id=1, replica_groups=mesh['dp'=4,'kv_0'=4,'kv_1'=4,'tp'=2] {'kv_0','tp'}, dimensions={0} | all-to-all | bytes 196608 | tf_op jit(solution)/shard_map/all_to_all | solution.py:360
  36.4 0.2 shard_map.172.part_ref
  36.6 0.3 shard_map.173
  37.0 10.8 %all_to_all.21 = bf16[16,32,256]{2,1,0:T(8,128)(2,1)S(1)} all-to-all(bf16[16,32,256]{2,1,0:T(8,128)(2,1)S(1)} %bitcast.22), channel_id=1, replica_groups=mesh['dp'=4,'kv_0'=4,'kv_1'=4,'tp'=2] {'kv_0','kv_1'}, dimensions={0} | all-to-all | bytes 524288 | tf_op jit(solution)/shard_map/all_to_all | solution.py:360
  47.8 0.6 gate_up.1
  48.4 2.3 %collective-permute-start.4 = (bf16[712,128]{1,0:T(8,128)(2,1)S(1)}, bf16[712,128]{1,0:T(8,128)(2,1)S(1)}, u32[]{:S(2)}, u32[]{:S(2)}) collective-permute-start(bf16[712,128]{1,0:T(8,128)(2,1)S(1)} %get-tuple-element.35), channel_id=1, source_target_pairs={{0,1},{1,0},{2,3},{3,2},{4,5},{5,4},{6,7},{7,6},{8,9},{9,8},{10,11... | collective-permute-start | bytes 546824 | tf_op jit(solution)/shard_map/ppermute | solution.py:355
  50.7 1.6 %update.1 = (f32[8,4,128,128]{3,2,1,0:T(8,128)}, f32[8,128]{1,0:T(8,128)S(1)}) custom-call(f32[8,4,128,128]{3,2,1,0:T(8,128)S(1)} %copy-done, f32[8,512]{1,0:T(8,128)S(1)} %get-tuple-element.36.key_ref, f32[8,512]{1,0:T(8,128)S(1)} %get-tuple-element.37.correct_ref, f32[8,128]{1,0:T(8,128)S(1)} %get-tuple-element.38.keep_ref, bf16[512,256]{1,0:T(8,128)(2,1)S(1)} %bitcast.21), custom_call_target="tpu_custom_call" | custom-call | tf_op jit(solution)/shard_map/update/pallas_call | solution.py:215
  52.3 0.5 shard_map.174
  52.7 11.1 %all_to_all.22 = bf16[16,64,128]{2,1,0:T(8,128)(2,1)S(1)} all-to-all(bf16[16,64,128]{2,1,0:T(8,128)(2,1)S(1)} %bitcast.24), channel_id=1, replica_groups=mesh['dp'=4,'kv_0'=4,'kv_1'=4,'tp'=2] {'kv_0','kv_1'}, dimensions={0} | all-to-all | bytes 524288 | tf_op jit(solution)/shard_map/all_to_all | solution.py:360
  63.8 0.6 %shard_map.175 = bf16[64,128]{1,0:T(8,128)(2,1)} custom-call(bf16[1024,128]{1,0:T(8,128)(2,1)S(1)} %bitcast.23, bf16[64,128]{1,0:T(8,128)(2,1)S(1)} %get-tuple-element.40.middle_ref), custom_call_target="tpu_custom_call" | custom-call | tf_op jit(solution)/shard_map/pallas_call | solution.py:444
  (15 shorter events, 0.1 us)
Async XLA Ops:
  0.6 2.9 %collective-permute-start.1 = (bf16[512,128]{1,0:T(8,128)(2,1)}, bf16[512,128]{1,0:T(8,128)(2,1)S(1)}, u32[]{:S(2)}, u32[]{:S(2)}) collective-permute-start(bf16[512,128]{1,0:T(8,128)(2,1)} %refs_9_.1), channel_id=1, source_target_pairs={{0,1},{1,0},{2,3},{3,2},{4,5},{5,4},{6,7},{7,6},{8,9},{9,8},{10,11... | collective-permute-start | bytes 393224 | tf_op jit(solution)/shard_map/ppermute | solution.py:355
  2.1 1.6 %collective-permute-start = (bf16[64,128]{1,0:T(8,128)(2,1)}, bf16[64,128]{1,0:T(8,128)(2,1)S(1)}, u32[]{:S(2)}, u32[]{:S(2)}) collective-permute-start(bf16[64,128]{1,0:T(8,128)(2,1)} %bitcast.33), channel_id=1, source_target_pairs={{0,1},{1,0},{2,3},{3,2},{4,5},{5,4},{6,7},{7,6},{8,9},{9,8},{10,11... | collective-permute-start | bytes 49160 | tf_op jit(solution)/shard_map/ppermute | solution.py:355
  3.5 22.1 %copy-start = (f32[8,4,128,128]{3,2,1,0:T(8,128)S(1)}, f32[8,4,128,128]{3,2,1,0:T(8,128)}, u32[]{:S(2)}) copy-start(f32[8,4,128,128]{3,2,1,0:T(8,128)} %state_ref.3) | copy-start | bytes 6291460
  3.5 22.1 %copy-start.4 = (f32[4]{0:T(128)S(1)}, f32[4]{0:T(128)}, u32[]{:S(2)}) copy-start(f32[4]{0:T(128)} %param.25) | copy-start | bytes 52
  3.5 22.1 %copy-start.5 = (f32[128]{0:T(128)S(1)}, f32[128]{0:T(128)}, u32[]{:S(2)}) copy-start(f32[128]{0:T(128)} %param.26) | copy-start | bytes 1540
  4.9 19.3 %all-to-all-start = ((bf16[16,8,2304]{2,1,0:T(8,128)(2,1)}), bf16[16,8,2304]{2,1,0:T(8,128)(2,1)S(1)}, u32[]{:S(2)}, u32[]{:S(2)}) async-start(bf16[16,8,2304]{2,1,0:T(8,128)(2,1)} %bitcast.5), calls=%async_computation | async-start | bytes 1179648 | tf_op jit(solution)/shard_map/all_to_all | solution.py:360
  12.8 12.8 %collective-permute-start.2 = (bf16[512,128]{1,0:T(8,128)(2,1)S(1)}, bf16[512,128]{1,0:T(8,128)(2,1)S(1)}, u32[]{:S(2)}, u32[]{:S(2)}) collective-permute-start(bf16[512,128]{1,0:T(8,128)(2,1)S(1)} %shard_map.167.after_ref.held_ref), channel_id=1, source_target_pairs={{0,6},{2,4},{4,2},{6,0},{1,7},{3,5},{5,3},{7,1},{8,14},{10,12},{12... | collective-permute-start | bytes 393224 | tf_op jit(solution)/shard_map/ppermute | solution.py:364
  25.5 11.1 %collective-permute-start.3 = (bf16[1024,128]{1,0:T(8,128)(2,1)S(1)}, bf16[1024,128]{1,0:T(8,128)(2,1)S(1)}, u32[]{:S(2)}, u32[]{:S(2)}) collective-permute-start(bf16[1024,128]{1,0:T(8,128)(2,1)S(1)} %shard_map.171.joined_ref), channel_id=1, source_target_pairs={{0,2},{2,0},{4,6},{6,4},{1,3},{3,1},{5,7},{7,5},{8,10},{10,8},{12,... | collective-permute-start | bytes 786440 | tf_op jit(solution)/shard_map/ppermute | solution.py:364
  25.7 22.1 %copy-start.1 = (bf16[1024,352]{0,1:T(8,128)(2,1)S(1)}, bf16[1024,352]{0,1:T(8,128)(2,1)}, u32[]{:S(2)}) copy-start(bf16[1024,352]{0,1:T(8,128)(2,1)} %param.29) | copy-start | bytes 2162692
  25.7 22.1 %copy-start.2 = (bf16[1024,352]{0,1:T(8,128)(2,1)S(1)}, bf16[1024,352]{0,1:T(8,128)(2,1)}, u32[]{:S(2)}) copy-start(bf16[1024,352]{0,1:T(8,128)(2,1)} %param.30) | copy-start | bytes 2162692
  47.8 4.5 %copy-start.3 = (bf16[352,1024]{1,0:T(8,128)(2,1)S(1)}, bf16[352,1024]{1,0:T(8,128)(2,1)}, u32[]{:S(2)}) copy-start(bf16[352,1024]{1,0:T(8,128)(2,1)} %w_ref.1) | copy-start | bytes 2162692
  48.4 3.9 %collective-permute-start.4 = (bf16[712,128]{1,0:T(8,128)(2,1)S(1)}, bf16[712,128]{1,0:T(8,128)(2,1)S(1)}, u32[]{:S(2)}, u32[]{:S(2)}) collective-permute-start(bf16[712,128]{1,0:T(8,128)(2,1)S(1)} %get-tuple-element.35), channel_id=1, source_target_pairs={{0,1},{1,0},{2,3},{3,2},{4,5},{5,4},{6,7},{7,6},{8,9},{9,8},{10,11... | collective-permute-start | bytes 546824 | tf_op jit(solution)/shard_map/ppermute | solution.py:355

commit v6 on v5

--- a/solution.py
+++ b/solution.py
@@ -143,7 +143,7 @@
     squares = sum(part * part for part in tokens)
     row_scale = lax.rsqrt(jnp.sum(squares, axis=1, keepdims=True) / D + norm_epsilon)
     small = small * row_scale
-    row = lax.broadcasted_iota(jnp.int32, (OWN, HEAD_DIM), 0)
+    own = jnp.bitwise_and(lax.broadcasted_iota(jnp.int32, (2 * OWN, HEAD_DIM), 0), OWN - 1)
     lane = lax.broadcasted_iota(jnp.int32, (OWN, HEAD_DIM), 1)
     keeps = jnp.zeros((OWN, HEAD_DIM), f32)
     low = lane < 64
@@ -172,13 +172,11 @@
         decay = small[:, HEADS_DEV + h : HEADS_DEV + h + 1]
         softplus = jnp.maximum(decay, 0.0) + jnp.log1p(jnp.exp(-jnp.abs(decay)))
         keep = jnp.exp(-rate_ref[:, h : h + 1] * softplus)
-        pair = jnp.concatenate([key, query], axis=0).astype(bf16)
-        recalled = jnp.zeros((OWN, HEAD_DIM), f32)
-        asked = jnp.zeros((OWN, HEAD_DIM), f32)
-        for b in range(OWN):
-            both = dot(pair, state_ref[b, h].astype(bf16))
-            recalled = jnp.where(row == b, both[:OWN], recalled)
-            asked = jnp.where(row == b, both[OWN:], asked)
+        pair = jnp.concatenate([key, query], axis=0)
+        spread = jnp.concatenate([jnp.where(own == b, pair, 0.0) for b in range(OWN)], axis=1)
+        states = state_ref[:, h].reshape(OWN * HEAD_DIM, HEAD_DIM)
+        both = dot(spread.astype(bf16), states.astype(bf16))
+        recalled, asked = both[:OWN], both[OWN:]
         correction = write_rate * (silu(value_lin) - keep * recalled)
         readout = keep * asked + jnp.sum(key * query, axis=1, keepdims=True) * correction
         readout = readout * lax.rsqrt(
@@ -279,17 +277,13 @@
     return parts
 
 
-def mix_near(received_ref, joined_ref, part_ref):
-    own, third = ring_parts(received_ref, joined_ref)
-    part_ref[:SEQ_RING] = own
-    part_ref[SEQ_RING:] = third
-
-
-def mix(received_ref, far_ref, part_ref, sent_ref):
+def mix(received_ref, joined_ref, far_ref, after_ref, sent_ref):
+    del after_ref
     place = lax.axis_index("kv_1")
     tokens = jnp.concatenate(ring_rows(received_ref, 0, WIDTH_DEV, MIXED), axis=0)
+    held, third = ring_parts(received_ref, joined_ref)
     first, second = ring_parts(received_ref, far_ref)
-    parts = [part_ref[:SEQ_RING], first, second, part_ref[SEQ_RING:]]
+    parts = [held, first, second, third]
 
     def part(column):
         which = jnp.bitwise_xor(place, column)
@@ -419,9 +413,9 @@
         [v] * 4,
     )(pieces, delta_state, decay_rate.reshape(1, HEADS_DEV), head_gain.reshape(1, HEAD_DIM))
     mixed_rows = over(mixed, ("kv_0", "tp"), 2 * RING)
-    near_part = kernel(mix_near, shape((2 * SEQ_RING, 128), f32), [v] * 2)(mixed_rows, joined)
-    sent = kernel(mix, shape((GROUP * SEQ_RING, FEAT_RING), bf16), [v] * 3)(
-        mixed_rows, far, near_part
+    arrived = kernel(note, shape((8, 128), f32), [a])(mixed_rows)
+    sent = kernel(mix, shape((GROUP * SEQ_RING, FEAT_RING), bf16), [v] * 3 + [a])(
+        mixed_rows, joined, far, arrived
     )
     received = over(sent, KV, GROUP)
     own_sum, sent_sum, middle = pl.pallas_call(

time: 64.8 us -> 64.5 us (level)
  transfers between devices with their start and end apart: 6 -> 6, of which waited for: 2 -> 2; matrix products, arithmetic and copies ran while one was open for 0% -> 0% of each run, Pallas kernels for 6% -> 5%
where the time goes in v6:
time: 64.5 us; the launch traced here: 64.2 us
  blocking collectives  32 us (50%)
  starting transfers between devices  14.4 us (22%)
  waiting for transfers between devices  10.2 us (16%)
  Pallas kernels  6.74 us (10%)
  between operations  0.8 us (1%)
    all_to_all x3, blocking collectives, over(): return lax.all_to_all(tiles, axes, 0, 0, tiled=True).reshape(array.shape)  32 us
    all_to_all x1, waiting for transfers between devices, over(): return lax.all_to_all(tiles, axes, 0, 0, tiled=True).reshape(array.shape)  8.81 us
    all_to_all x1, starting transfers between devices, over(): return lax.all_to_all(tiles, axes, 0, 0, tiled=True).reshape(array.shape)  7.88 us
    ppermute x3, starting transfers between devices, from_other_core(): return lax.ppermute(array, 'tp', [(0, 1), (1, 0)])  3.87 us
    ppermute x2, starting transfers between devices, from_ring(): return lax.ppermute(array, 'kv_1', [(i, i ^ flip) for i in range(RING)])  2.66 us
    pallas_call x1, Pallas kernels, updated(): pl.pallas_call(update, out_shape=[shape(operands[0].shape, f32), shape((8...  1.56 us
    ppermute x2, waiting for transfers between devices, from_ring(): return lax.ppermute(array, 'kv_1', [(i, i ^ flip) for i in range(RING)])  1.38 us
    pallas_call x1, Pallas kernels, preloaded(): pl.pallas_call(preload, out_shape=[shape(x.shape, x.dtype) for x in array...  1.31 us
  transfers between devices with their start and end apart: 6, of which 2 were waited for; matrix products, arithmetic and copies ran while one was open for 0% of the time, Pallas kernels for 5%

profile of v6, /device:TPU:1, one launch (start us, length us, event | category | flops | bytes accessed | tf_op | source)
XLA Modules:
  0.0 64.2 jit_solution(12559193581834263175)
XLA Ops:
  0.6 1.5 %collective-permute-start.1 = (bf16[512,128]{1,0:T(8,128)(2,1)}, bf16[512,128]{1,0:T(8,128)(2,1)S(1)}, u32[]{:S(2)}, u32[]{:S(2)}) collective-permute-start(bf16[512,128]{1,0:T(8,128)(2,1)} %refs_9_.1), channel_id=1, source_target_pairs={{0,1},{1,0},{2,3},{3,2},{4,5},{5,4},{6,7},{7,6},{8,9},{9,8},{10,11... | collective-permute-start | bytes 393224 | tf_op jit(solution)/shard_map/ppermute | solution.py:349
  2.1 0.1 collective-permute-start
  2.2 1.3 %preload.1 = (bf16[64,128]{1,0:T(8,128)(2,1)S(1)}, bf16[1,128]{1,0:T(2,128)(2,1)S(1)}, bf16[1,128]{1,0:T(2,128)(2,1)S(1)}, bf16[128,512]{1,0:T(8,128)(2,1)S(1)},...) custom-call(bf16[64,128]{1,0:T(8,128)(2,1)} %bitcast.34, ...), custom_call_target="tpu_custom_call" | custom-call | tf_op jit(solution)/shard_map/preload/pallas_call | solution.py:240
  3.5 0.0 copy-start
  3.5 0.0 copy-start.4
  3.5 0.0 copy-start.5
  3.6 0.1 shard_map.167.after_ref.held_ref
  3.7 1.2 %shard_map.168 = bf16[128,2304]{1,0:T(8,128)(2,1)} custom-call(bf16[64,128]{1,0:T(8,128)(2,1)S(1)} %get-tuple-element.22.own_ref, bf16[1,128]{1,0:T(2,128)(2,1)S(1)} %get-tuple-element.23.gain_ref, bf16[1,128]{1,0:T(2,128)(2,1)S(1)} %get-tuple-element.24.gain_mid_ref, bf16[128,512]{1,0:T(8,128)(2,1)S(1)} %get-tuple-element.25.wq_ref, ...), custom_call_target="tpu_custom_call" | custom-call | tf_op jit(solution)/shard_map/pallas_call | solution.py:397
  4.9 7.9 %all-to-all-start = ((bf16[16,8,2304]{2,1,0:T(8,128)(2,1)}), bf16[16,8,2304]{2,1,0:T(8,128)(2,1)S(1)}, u32[]{:S(2)}, u32[]{:S(2)}) async-start(bf16[16,8,2304]{2,1,0:T(8,128)(2,1)} %bitcast.5), calls=%async_computation | async-start | bytes 1179648 | tf_op jit(solution)/shard_map/all_to_all | solution.py:354
  12.8 2.6 %collective-permute-start.2 = (bf16[512,128]{1,0:T(8,128)(2,1)S(1)}, bf16[512,128]{1,0:T(8,128)(2,1)S(1)}, u32[]{:S(2)}, u32[]{:S(2)}) collective-permute-start(bf16[512,128]{1,0:T(8,128)(2,1)S(1)} %shard_map.167.after_ref.held_ref), channel_id=1, source_target_pairs={{0,6},{2,4},{4,2},{6,0},{1,7},{3,5},{5,3},{7,1},{8,14},{10,12},{12... | collective-permute-start | bytes 393224 | tf_op jit(solution)/shard_map/ppermute | solution.py:358
  15.3 8.8 %all-to-all-done = bf16[16,8,2304]{2,1,0:T(8,128)(2,1)S(1)} async-done(((bf16[16,8,2304]{2,1,0:T(8,128)(2,1)}), bf16[16,8,2304]{2,1,0:T(8,128)(2,1)S(1)}, u32[]{:S(2)}, u32[]{:S(2)}) %all-to-all-start) | async-done | bytes 589856 | tf_op jit(solution)/shard_map/all_to_all | solution.py:354
  24.1 1.4 %collective-permute-done.2.near_ref = bf16[512,128]{1,0:T(8,128)(2,1)S(1)} collective-permute-done((bf16[512,128]{1,0:T(8,128)(2,1)S(1)}, bf16[512,128]{1,0:T(8,128)(2,1)S(1)}, u32[]{:S(2)}, u32[]{:S(2)}) %collective-permute-start.2) | collective-permute-done | bytes 131104 | tf_op jit(solution)/shard_map/ppermute | solution.py:358
  25.5 0.1 collective-permute-start.3
  25.7 0.0 copy-start.1
  25.7 0.5 shard_map.169
  26.2 10.0 %all_to_all.20 = bf16[8,8,768]{2,1,0:T(8,128)(2,1)S(1)} all-to-all(bf16[8,8,768]{2,1,0:T(8,128)(2,1)S(1)} %bitcast.29), channel_id=1, replica_groups=mesh['dp'=4,'kv_0'=4,'kv_1'=4,'tp'=2] {'kv_0','tp'}, dimensions={0} | all-to-all | bytes 196608 | tf_op jit(solution)/shard_map/all_to_all | solution.py:354
  36.2 0.4 shard_map.173
  36.6 10.8 %all_to_all.21 = bf16[16,32,256]{2,1,0:T(8,128)(2,1)S(1)} all-to-all(bf16[16,32,256]{2,1,0:T(8,128)(2,1)S(1)} %bitcast.22), channel_id=1, replica_groups=mesh['dp'=4,'kv_0'=4,'kv_1'=4,'tp'=2] {'kv_0','kv_1'}, dimensions={0} | all-to-all | bytes 524288 | tf_op jit(solution)/shard_map/all_to_all | solution.py:354
  47.5 0.6 gate_up.1
  48.0 2.3 %collective-permute-start.4 = (bf16[712,128]{1,0:T(8,128)(2,1)S(1)}, bf16[712,128]{1,0:T(8,128)(2,1)S(1)}, u32[]{:S(2)}, u32[]{:S(2)}) collective-permute-start(bf16[712,128]{1,0:T(8,128)(2,1)S(1)} %get-tuple-element.35), channel_id=1, source_target_pairs={{0,1},{1,0},{2,3},{3,2},{4,5},{5,4},{6,7},{7,6},{8,9},{9,8},{10,11... | collective-permute-start | bytes 546824 | tf_op jit(solution)/shard_map/ppermute | solution.py:349
  50.3 1.6 %update.1 = (f32[8,4,128,128]{3,2,1,0:T(8,128)}, f32[8,128]{1,0:T(8,128)S(1)}) custom-call(f32[8,4,128,128]{3,2,1,0:T(8,128)S(1)} %copy-done, f32[8,512]{1,0:T(8,128)S(1)} %get-tuple-element.36.key_ref, f32[8,512]{1,0:T(8,128)S(1)} %get-tuple-element.37.correct_ref, f32[8,128]{1,0:T(8,128)S(1)} %get-tuple-element.38.keep_ref, bf16[512,256]{1,0:T(8,128)(2,1)S(1)} %bitcast.21), custom_call_target="tpu_custom_call" | custom-call | tf_op jit(solution)/shard_map/update/pallas_call | solution.py:213
  51.9 0.4 shard_map.174
  52.4 11.1 %all_to_all.22 = bf16[16,64,128]{2,1,0:T(8,128)(2,1)S(1)} all-to-all(bf16[16,64,128]{2,1,0:T(8,128)(2,1)S(1)} %bitcast.24), channel_id=1, replica_groups=mesh['dp'=4,'kv_0'=4,'kv_1'=4,'tp'=2] {'kv_0','kv_1'}, dimensions={0} | all-to-all | bytes 524288 | tf_op jit(solution)/shard_map/all_to_all | solution.py:354
  63.5 0.6 %shard_map.175 = bf16[64,128]{1,0:T(8,128)(2,1)} custom-call(bf16[1024,128]{1,0:T(8,128)(2,1)S(1)} %bitcast.23, bf16[64,128]{1,0:T(8,128)(2,1)S(1)} %get-tuple-element.40.middle_ref), custom_call_target="tpu_custom_call" | custom-call | tf_op jit(solution)/shard_map/pallas_call | solution.py:438
  (15 shorter events, 0.0 us)
Async XLA Ops:
  0.6 2.9 %collective-permute-start.1 = (bf16[512,128]{1,0:T(8,128)(2,1)}, bf16[512,128]{1,0:T(8,128)(2,1)S(1)}, u32[]{:S(2)}, u32[]{:S(2)}) collective-permute-start(bf16[512,128]{1,0:T(8,128)(2,1)} %refs_9_.1), channel_id=1, source_target_pairs={{0,1},{1,0},{2,3},{3,2},{4,5},{5,4},{6,7},{7,6},{8,9},{9,8},{10,11... | collective-permute-start | bytes 393224 | tf_op jit(solution)/shard_map/ppermute | solution.py:349
  2.1 1.6 %collective-permute-start = (bf16[64,128]{1,0:T(8,128)(2,1)}, bf16[64,128]{1,0:T(8,128)(2,1)S(1)}, u32[]{:S(2)}, u32[]{:S(2)}) collective-permute-start(bf16[64,128]{1,0:T(8,128)(2,1)} %bitcast.33), channel_id=1, source_target_pairs={{0,1},{1,0},{2,3},{3,2},{4,5},{5,4},{6,7},{7,6},{8,9},{9,8},{10,11... | collective-permute-start | bytes 49160 | tf_op jit(solution)/shard_map/ppermute | solution.py:349
  3.5 22.1 %copy-start = (f32[8,4,128,128]{3,2,1,0:T(8,128)S(1)}, f32[8,4,128,128]{3,2,1,0:T(8,128)}, u32[]{:S(2)}) copy-start(f32[8,4,128,128]{3,2,1,0:T(8,128)} %state_ref.3) | copy-start | bytes 6291460
  3.5 22.1 %copy-start.4 = (f32[4]{0:T(128)S(1)}, f32[4]{0:T(128)}, u32[]{:S(2)}) copy-start(f32[4]{0:T(128)} %param.25) | copy-start | bytes 52
  3.5 22.1 %copy-start.5 = (f32[128]{0:T(128)S(1)}, f32[128]{0:T(128)}, u32[]{:S(2)}) copy-start(f32[128]{0:T(128)} %param.26) | copy-start | bytes 1540
  4.9 19.3 %all-to-all-start = ((bf16[16,8,2304]{2,1,0:T(8,128)(2,1)}), bf16[16,8,2304]{2,1,0:T(8,128)(2,1)S(1)}, u32[]{:S(2)}, u32[]{:S(2)}) async-start(bf16[16,8,2304]{2,1,0:T(8,128)(2,1)} %bitcast.5), calls=%async_computation | async-start | bytes 1179648 | tf_op jit(solution)/shard_map/all_to_all | solution.py:354
  12.8 12.8 %collective-permute-start.2 = (bf16[512,128]{1,0:T(8,128)(2,1)S(1)}, bf16[512,128]{1,0:T(8,128)(2,1)S(1)}, u32[]{:S(2)}, u32[]{:S(2)}) collective-permute-start(bf16[512,128]{1,0:T(8,128)(2,1)S(1)} %shard_map.167.after_ref.held_ref), channel_id=1, source_target_pairs={{0,6},{2,4},{4,2},{6,0},{1,7},{3,5},{5,3},{7,1},{8,14},{10,12},{12... | collective-permute-start | bytes 393224 | tf_op jit(solution)/shard_map/ppermute | solution.py:358
  25.5 10.7 %collective-permute-start.3 = (bf16[1024,128]{1,0:T(8,128)(2,1)S(1)}, bf16[1024,128]{1,0:T(8,128)(2,1)S(1)}, u32[]{:S(2)}, u32[]{:S(2)}) collective-permute-start(bf16[1024,128]{1,0:T(8,128)(2,1)S(1)} %shard_map.171.joined_ref), channel_id=1, source_target_pairs={{0,2},{2,0},{4,6},{6,4},{1,3},{3,1},{5,7},{7,5},{8,10},{10,8},{12,... | collective-permute-start | bytes 786440 | tf_op jit(solution)/shard_map/ppermute | solution.py:358
  25.7 21.8 %copy-start.1 = (bf16[1024,352]{0,1:T(8,128)(2,1)S(1)}, bf16[1024,352]{0,1:T(8,128)(2,1)}, u32[]{:S(2)}) copy-start(bf16[1024,352]{0,1:T(8,128)(2,1)} %param.29) | copy-start | bytes 2162692
  25.7 21.8 %copy-start.2 = (bf16[1024,352]{0,1:T(8,128)(2,1)S(1)}, bf16[1024,352]{0,1:T(8,128)(2,1)}, u32[]{:S(2)}) copy-start(bf16[1024,352]{0,1:T(8,128)(2,1)} %param.30) | copy-start | bytes 2162692
  47.5 4.5 %copy-start.3 = (bf16[352,1024]{1,0:T(8,128)(2,1)S(1)}, bf16[352,1024]{1,0:T(8,128)(2,1)}, u32[]{:S(2)}) copy-start(bf16[352,1024]{1,0:T(8,128)(2,1)} %w_ref.1) | copy-start | bytes 2162692
  48.0 3.9 %collective-permute-start.4 = (bf16[712,128]{1,0:T(8,128)(2,1)S(1)}, bf16[712,128]{1,0:T(8,128)(2,1)S(1)}, u32[]{:S(2)}, u32[]{:S(2)}) collective-permute-start(bf16[712,128]{1,0:T(8,128)(2,1)S(1)} %get-tuple-element.35), channel_id=1, source_target_pairs={{0,1},{1,0},{2,3},{3,2},{4,5},{5,4},{6,7},{7,6},{8,9},{9,8},{10,11... | collective-permute-start | bytes 546824 | tf_op jit(solution)/shard_map/ppermute | solution.py:349
